TPU v7x, 32 devices: a whole 2x2x4 slice. The times are simulated.
32 devices in a mesh: sp: 4 (over z), fs: 4 (over y, core), tp: 2 (over x).
Axes of the slice: x: 2, y: 2, z: 4, core: 2. Of those that a mesh axis runs over, the one named last changes fastest.
Arguments:
- input_layer_rows: bfloat16 [4, 1024, 2048], P('fs', 'sp'), may hold values from -6 to 6
- input_norm_gain: float32 [2048], replicated, may hold values from 0.1 to 1.9
- query_weight_attention: bfloat16 [2048, 1024], P(('sp', 'fs'), 'tp'), may hold values from -0.125 to 0.125
- key_weight_attention: bfloat16 [2048, 1024], P(('sp', 'fs'), 'tp'), may hold values from -0.125 to 0.125
- value_weight_attention: bfloat16 [2048, 1024], P(('sp', 'fs'), 'tp'), may hold values from -0.125 to 0.125
- query_weight_recurrent: bfloat16 [2048, 1024], P(('sp', 'fs'), 'tp'), may hold values from -0.125 to 0.125
- forget_weight_recurrent: bfloat16 [2048, 1024], P(('sp', 'fs'), 'tp'), may hold values from -0.125 to 0.125
- value_weight_recurrent: bfloat16 [2048, 1024], P(('sp', 'fs'), 'tp'), may hold values from -0.125 to 0.125
- gate_weight_recurrent: bfloat16 [2048, 1024], P(('sp', 'fs'), 'tp'), may hold values from -0.125 to 0.125
- output_weight_attention: bfloat16 [2048, 1024], P(('sp', 'fs'), 'tp'), may hold values from -0.125 to 0.125
- emitted_projection_linear_scan: bfloat16 [2048, 1024], P(('sp', 'fs'), 'tp'), may hold values from -0.125 to 0.125
- score_offset: float32 [8], P('tp'), as said below
- attention_norm_gain: float32 [1024], P('tp'), may hold values from 0.1 to 1.9
- recurrence_norm_gain: float32 [1024], P('tp'), may hold values from 0.1 to 1.9
- forget_floor: float32 [1024], P('tp'), may hold values from 0.1 to 0.5
- forget_offset: float32 [1024], P('tp'), as said below
- extra_log_decay: float32 [4, 1024, 1024], P('fs', 'sp', 'tp')
Outputs:
- layer_out: bfloat16 [4, 1024, 2048], P('fs', ('sp', 'tp'))
- row_log_total: float32 [4, 8, 1024], P('fs', 'tp', 'sp')
Inputs may be any that keep to these rules, and one draw needn't show every extreme that they name: `score_offset`: each head's offset lies between -ln(1024) - 2 and -ln(1024) + 0.5. `forget_offset`: each channel's offset lies between ln(256) - 3 and ln(1024) + 0.6.
All inputs are finite; a program needn't handle non-finite values.
Results may differ from a plain program's by a relative error of at most 0.015.
Values may be sent and summed in bfloat16 or wider, within the bound.
A program may use at most 64 MiB of HBM per device.

v0:
```python
import jax
import jax.numpy as jnp
from jax import lax
from jax.sharding import PartitionSpec as P

HEAD = 128
BLOCK = 64


epsilon = 1e-06
log_floor = 0.05


def entering(shard, axis, combine, identity):
    size, index = (lax.axis_size(axis), lax.axis_index(axis))
    everything = jax.tree.map(
        lambda part, kind: lax.all_gather(part.astype(kind), axis),
        shard,
        (jnp.bfloat16, jnp.bfloat16),
    )
    start = jax.tree.map(
        lambda part, zero: jnp.broadcast_to(jnp.asarray(zero, part.dtype), part.shape),
        shard,
        identity,
    )

    def hop(k, before):
        reached = k < index
        new = combine(
            before, jax.tree.map(lambda part, own: part[k].astype(own.dtype), everything, shard)
        )
        return jax.tree.map(lambda a, b: jnp.where(reached, a, b), new, before)

    return lax.fori_loop(0, size, hop, start)


def head_norm(values, gain):
    square_mean = jnp.mean(values * values, axis=-1, keepdims=True)
    return values * lax.rsqrt(square_mean + epsilon) * gain


def recurrence_block(memory_matrix, inputs):
    query_slice, decay_part, key_slice, value_slice = inputs
    highest_score = lax.Precision.HIGHEST
    length = decay_part.shape[0]
    running_total = jnp.cumsum(decay_part, axis=0)
    causal = (
        lax.broadcasted_iota(jnp.int32, (length, length), 0)
        >= lax.broadcasted_iota(jnp.int32, (length, length), 1)
    )[:, :, None, None]
    relative = jnp.where(causal, running_total[:, None] - running_total[None, :], -jnp.inf)
    pairwise = jnp.sum(query_slice[:, None] * key_slice[None, :] * jnp.exp(relative), axis=-1)
    inner_part = jnp.einsum("tsh,shv->thv", pairwise, value_slice, precision=highest_score)
    carried_state = jnp.einsum(
        "fby,bym->fbm", query_slice * jnp.exp(running_total), memory_matrix, precision=highest_score
    )
    final_total = running_total[-1]
    updated_state = jnp.exp(final_total)[:, :, None] * memory_matrix + jnp.einsum(
        "rxc,rxa->xca",
        key_slice * jnp.exp(final_total[None] - running_total),
        value_slice,
        precision=highest_score,
    )
    return (updated_state, inner_part + carried_state)


def stick_piece(queries, shifts, weighted, keep_total, key_value, is_own, is_valid):
    scores = (
        jnp.einsum("thd,shd->hts", queries, key_value[0], preferred_element_type=jnp.float32)
        * HEAD ** (-0.5)
        + shifts[:, None, None]
    )
    logarithmic_retention = jax.nn.log_sigmoid(-scores)
    if is_own:
        rows_here = scores.shape[1]
        strict = lax.broadcasted_iota(jnp.int32, (rows_here, rows_here), 0) > lax.broadcasted_iota(
            jnp.int32, (rows_here, rows_here), 1
        )
        logarithmic_retention = jnp.where(strict, logarithmic_retention, 0.0)
    suffix = lax.cumsum(logarithmic_retention, axis=2, reverse=True) - logarithmic_retention
    log_weight = jax.nn.log_sigmoid(scores) + suffix + keep_total[:, :, None]
    if is_own:
        log_weight = jnp.where(strict, log_weight, -jnp.inf)
    weights = jnp.where(is_valid, jnp.exp(log_weight), 0.0).astype(jnp.bfloat16)
    weighted = weighted + jnp.einsum(
        "hts,shd->thd", weights, key_value[1], preferred_element_type=jnp.float32
    )
    keep_total = keep_total + jnp.where(is_valid, jnp.sum(logarithmic_retention, axis=2), 0.0)
    return (weighted, keep_total)


def contract_rows(rows_in, weight):
    return lax.dot_general(
        rows_in, weight, (((1,), (1,)), ((), ())), preferred_element_type=jnp.float32
    )


def on_device(
    input_layer_rows,
    input_norm_gain,
    query_weight_attention,
    key_weight_attention,
    value_weight_attention,
    query_weight_recurrent,
    forget_weight_recurrent,
    value_weight_recurrent,
    gate_weight_recurrent,
    output_weight_attention,
    emitted_projection_linear_scan,
    score_offset,
    attention_norm_gain,
    recurrence_norm_gain,
    forget_floor,
    forget_offset,
    extra_log_decay,
):
    values = input_layer_rows[0].astype(jnp.float32)
    square_mean = jnp.mean(values * values, axis=-1, keepdims=True)
    normed = (values * lax.rsqrt(square_mean + epsilon) * input_norm_gain).astype(jnp.bfloat16)
    tokens = normed.shape[0]
    weights_in = (
        query_weight_attention,
        key_weight_attention,
        value_weight_attention,
        query_weight_recurrent,
        forget_weight_recurrent,
        value_weight_recurrent,
        gate_weight_recurrent,
    )
    pieces = (
        lax.all_gather(weights_in[0], ("sp", "fs"), axis=0, tiled=True),
        lax.all_gather(weights_in[1], ("sp", "fs"), axis=0, tiled=True),
        lax.all_gather(weights_in[2], ("sp", "fs"), axis=0, tiled=True),
        lax.all_gather(weights_in[3], ("sp", "fs"), axis=0, tiled=True),
        lax.all_gather(weights_in[4], ("sp", "fs"), axis=0, tiled=True),
        lax.all_gather(weights_in[5], ("sp", "fs"), axis=0, tiled=True),
        lax.all_gather(weights_in[6], ("sp", "fs"), axis=0, tiled=True),
    )
    projected = tuple(
        (jnp.dot(normed, weight, preferred_element_type=jnp.float32) for weight in pieces)
    )
    query_a, key_a, value_a, query_b, forget_b, input_b, gate_b = [
        column_block.astype(jnp.bfloat16) for column_block in projected
    ]
    out_a, out_b = (
        lax.all_gather(output_weight_attention, ("sp", "fs"), axis=0, tiled=True),
        lax.all_gather(emitted_projection_linear_scan, ("sp", "fs"), axis=0, tiled=True),
    )
    head_count = query_a.shape[1] // HEAD
    queries = query_a.reshape(tokens, head_count, HEAD)
    key_value = jnp.stack(
        [key_a.reshape(tokens, head_count, HEAD), value_a.reshape(tokens, head_count, HEAD)]
    )
    weighted = jnp.zeros((tokens, head_count, HEAD), jnp.float32)
    keep_total = jnp.zeros((head_count, tokens), jnp.float32)
    weighted, keep_total = stick_piece(
        queries, score_offset, weighted, keep_total, key_value, True, True
    )
    position = lax.axis_index("sp")
    seq_devices = lax.axis_size("sp")
    gathered = lax.all_gather(key_value, "sp", axis=1, tiled=True)

    def gathered_turn(turn_index, carried_state):
        weighted_now, keep_now = carried_state
        source = jnp.maximum(position - turn_index, 0) * tokens
        piece_pair = lax.dynamic_slice_in_dim(gathered, source, tokens, 1)
        return stick_piece(
            queries, score_offset, weighted_now, keep_now, piece_pair, False, position >= turn_index
        )

    weighted, keep_total = lax.fori_loop(1, seq_devices, gathered_turn, (weighted, keep_total))
    row_log_total = jnp.log(jnp.maximum(-jnp.expm1(keep_total), log_floor))[None]
    mixed_a = (
        head_norm(weighted, attention_norm_gain.reshape(head_count, HEAD))
        .reshape(tokens, head_count * HEAD)
        .astype(jnp.bfloat16)
    )
    forget_logits = forget_b.astype(jnp.float32) + forget_offset
    forget_log_value = (
        jnp.logaddexp(
            jnp.log(forget_floor), jnp.log1p(-forget_floor) + jax.nn.log_sigmoid(forget_logits)
        )
        + extra_log_decay[0]
    )
    key_in = (1.0 - forget_floor) * jax.nn.sigmoid(-forget_logits)
    query_rows_input = jax.nn.silu(query_b.astype(jnp.float32)).reshape(tokens, head_count, HEAD)
    value_in = input_b.astype(jnp.float32)
    fading_channel_groups = forget_log_value.reshape(tokens, head_count, HEAD)
    shaped = tuple(
        (
            array_in.reshape(tokens // BLOCK, BLOCK, head_count, HEAD)
            for array_in in (query_rows_input, forget_log_value, key_in, value_in)
        )
    )
    empty_state = jnp.zeros((head_count, HEAD, HEAD), jnp.float32)
    nearby_hidden_vector, local_out = lax.scan(recurrence_block, empty_state, shaped)
    local_out = local_out.reshape(tokens, head_count, HEAD)
    through = jnp.exp(jnp.sum(fading_channel_groups, axis=0))

    def chain_states(earlier, later):
        return (earlier[0] * later[0], later[0][:, :, None] * earlier[1] + later[1])

    identity = (jnp.ones_like(through), jnp.zeros_like(nearby_hidden_vector))
    unused_decay, incoming_state = entering(
        (through, nearby_hidden_vector), "sp", chain_states, identity
    )
    running_sum = jnp.cumsum(fading_channel_groups, axis=0)
    recurrent = local_out + jnp.einsum(
        "fby,bym->fbm",
        query_rows_input * jnp.exp(running_sum),
        incoming_state,
        precision=lax.Precision.HIGHEST,
    )
    gated_out = head_norm(recurrent, recurrence_norm_gain.reshape(head_count, HEAD)) * jax.nn.silu(
        gate_b.astype(jnp.float32).reshape(tokens, head_count, HEAD)
    )
    mixed_b = gated_out.reshape(tokens, head_count * HEAD).astype(jnp.bfloat16)
    summed = lax.psum_scatter(
        (contract_rows(mixed_a, out_a) + contract_rows(mixed_b, out_b)).astype(jnp.bfloat16),
        "tp",
        scatter_dimension=0,
        tiled=True,
    )
    layer_out = summed[None]
    return (layer_out, row_log_total)


def solution(mesh):
    return jax.shard_map(
        on_device,
        mesh=mesh,
        in_specs=(
            P("fs", "sp", None),
            P(),
            P(("sp", "fs"), "tp"),
            P(("sp", "fs"), "tp"),
            P(("sp", "fs"), "tp"),
            P(("sp", "fs"), "tp"),
            P(("sp", "fs"), "tp"),
            P(("sp", "fs"), "tp"),
            P(("sp", "fs"), "tp"),
            P(("sp", "fs"), "tp"),
            P(("sp", "fs"), "tp"),
            P("tp"),
            P("tp"),
            P("tp"),
            P("tp"),
            P("tp"),
            P("fs", "sp", "tp"),
        ),
        out_specs=(P("fs", ("sp", "tp"), None), P("fs", "tp", "sp")),
        check_vma=False,
    )
```

profile of v0, /device:TPU:0, one launch (start us, length us, event | category | flops | bytes accessed | tf_op | source)
XLA Modules:
  0.0 472.7 jit_solution(9286617565874748095)
XLA Ops:
  13.5 40.9 %all-gather.16.cloned.1.call-done = bf16[2048,512]{1,0:T(8,128)(2,1)} async-done(((bf16[128,512]{1,0:T(8,128)(2,1)}), bf16[2048,512]{1,0:T(8,128)(2,1)}) %all-gather.16.cloned.1.call-update) | async-done | bytes 2097168 | tf_op jit(solution)/shard_map/all_gather | solution.py:132
  54.3 2.7 convolution_convert_fusion.4
  57.8 38.9 %all-gather.12.cloned.1.call-done = bf16[2048,512]{1,0:T(8,128)(2,1)} async-done(((bf16[128,512]{1,0:T(8,128)(2,1)}), bf16[2048,512]{1,0:T(8,128)(2,1)}) %all-gather.12.cloned.1.call-update) | async-done | bytes 2097168 | tf_op jit(solution)/shard_map/all_gather | solution.py:133
  96.7 2.3 convolution_convert_fusion.6
  102.2 36.9 %all-gather.22.cloned.1.call-done = bf16[2048,512]{1,0:T(8,128)(2,1)} async-done(((bf16[128,512]{1,0:T(8,128)(2,1)}), bf16[2048,512]{1,0:T(8,128)(2,1)}) %all-gather.22.cloned.1.call-update) | async-done | bytes 2097168 | tf_op jit(solution)/shard_map/all_gather | solution.py:135
  139.1 3.1 fusion.67
  143.6 37.7 %all-gather.26.cloned.1.call-done = bf16[2048,512]{1,0:T(8,128)(2,1)} async-done(((bf16[128,512]{1,0:T(8,128)(2,1)}), bf16[2048,512]{1,0:T(8,128)(2,1)}) %all-gather.26.cloned.1.call-update) | async-done | bytes 2097168 | tf_op jit(solution)/shard_map/all_gather | solution.py:134
  181.3 2.8 divide_multiply_fusion
  184.3 39.2 %all-gather.24.cloned.1.call-done = bf16[2048,512]{1,0:T(8,128)(2,1)} async-done(((bf16[128,512]{1,0:T(8,128)(2,1)}), bf16[2048,512]{1,0:T(8,128)(2,1)}) %all-gather.24.cloned.1.call-update) | async-done | bytes 2097168 | tf_op jit(solution)/shard_map/all_gather | solution.py:136
  223.5 2.7 fusion.39
  226.4 24.0 %while.43 = (s32[]{:T(128)}, f32[4,128,128]{2,1,0:T(8,128)S(1)}, f32[4,64,4,128]{3,1,0,2:T(8,128)}, f32[4,64,4,128]{3,2,1,0:T(4,128)S(1)}, f32[4,64,4,128]{3,2,1...) while((s32[]{:T(128)}, f32[4,128,128]{2,1,0:T(8,128)S(1)}, ...), condition=%wide.region_13.14_spmd.clone, body=%wide.region_10.13_spmd.clone.sunk | while | flops 138760192 | bytes 4346484 | solution.py:196
  226.7 3.7 multiply_reduce_fusion.4
  232.7 3.7 multiply_reduce_fusion.4
  238.7 3.7 multiply_reduce_fusion.4
  244.7 3.7 multiply_reduce_fusion.4
  250.5 20.1 %all-gather = bf16[16,128,128]{2,1,0:T(8,128)(2,1)S(1)} all-gather(bf16[4,128,128]{2,1,0:T(8,128)(2,1)S(1)} %convert_element_type.119), channel_id=2, replica_groups=mesh['sp'=4,'fs'=4,'tp'=2] {'sp'}, dimensions={0}, use_global_device_ids=true | all-gather | bytes 655360 | tf_op jit(solution)/shard_map/all_gather | solution.py:17
  270.6 9.2 %all_gather.48 = bf16[4,4,128]{2,1,0:T(4,128)(2,1)S(1)} all-gather(bf16[1,4,128]{2,1,0:T(4,128)(2,1)S(1)} %fusion.58), channel_id=1, replica_groups=mesh['sp'=4,'fs'=4,'tp'=2] {'sp'}, dimensions={0}, use_global_device_ids=true | all-gather | bytes 5120 | tf_op jit(solution)/shard_map/all_gather | solution.py:17
  279.8 12.2 %while.44 = (s32[]{:T(128)}, f32[4,128,128]{2,1,0:T(8,128)S(1)}, s32[]{:T(128)}, bf16[4,4,128]{2,1,0:T(4,128)(2,1)S(1)}, bf16[4,4,128,128]{3,2,1,0:T(8,128)(2,1)S(1)}, /*index=5*/s32[]{:T(128)}, s32[]{:T(128)}) while((s32[]{:T(128)}, f32[4,128,128]{2,1,0:T(8,128)S(1)}, s32[]{:T(128)}, bf16[4,4,128]{2,1,0:T(4,128)(2,1)S(1)}, ...), condition=%wide.region_16.17_spmd.clone, body=%wide.region_15.16_spmd.clone.sunk | while | flops 328196 | bytes 660585 | solution.py:34
  294.5 2.5 fusion.41
  297.3 14.6 %all-gather.14.cloned.1.call-done = bf16[2048,512]{1,0:T(8,128)(2,1)} async-done(((bf16[128,512]{1,0:T(8,128)(2,1)}), bf16[2048,512]{1,0:T(8,128)(2,1)}) %all-gather.14.cloned.1.call-update) | async-done | bytes 2097168 | tf_op jit(solution)/shard_map/all_gather | solution.py:131
  311.9 2.3 fusion.42
  316.2 9.2 %fusion.48 = f32[4,256,2,128]{1,2,3,0:T(2,128)S(1)} fusion(f32[4,256,2,128]{1,3,2,0:T(8,128)S(1)} %bitcast.197), kind=kOutput, calls=%fused_computation.90 | output fusion | flops 33292288 | bytes 2097152 | tf_op jit(solution)/shard_map/reduce-window
  328.6 29.9 %all-gather.18.cloned.1.call-done = bf16[2,1024,4,128]{3,1,2,0:T(8,128)(2,1)} async-done(((bf16[2,256,4,128]{3,1,2,0:T(8,128)(2,1)}), bf16[2,1024,4,128]{3,1,2,0:T(8,128)(2,1)}) %all-gather.18.cloned.1.call-update) | async-done | bytes 2097168 | tf_op jit(solution)/shard_map/all_gather | solution.py:161
  358.5 43.2 %while.42 = (s32[]{:T(128)}, f32[256,4,128]{0,2,1:T(8,128)S(1)}, f32[4,256]{1,0:T(4,128)S(1)}, s32[]{:T(128)}, bf16[2,1024,4,128]{3,1,2,0:T(8,128)(2,1)}, /*inde...) while((s32[]{:T(128)}, f32[256,4,128]{0,2,1:T(8,128)S(1)}, ...), condition=%wide.region_8.9_spmd, body=%wide.region_4.8_spmd.sunk | while | flops 175772672 | bytes 13451514 | solution.py:171
  360.4 9.2 %fusion.108 = f32[4,256,2,128]{1,2,3,0:T(2,128)S(1)} fusion(f32[4,256,2,128]{1,3,2,0:T(8,128)S(1)} %bitcast.196), kind=kOutput, calls=%fused_computation.14.clone.1 | output fusion | flops 33292288 | bytes 2097152 | tf_op jit(solution)/shard_map/reduce-window.8
  372.9 1.9 fusion.107
  374.8 9.2 %fusion.108 = f32[4,256,2,128]{1,2,3,0:T(2,128)S(1)} fusion(f32[4,256,2,128]{1,3,2,0:T(8,128)S(1)} %bitcast.196), kind=kOutput, calls=%fused_computation.14.clone.1 | output fusion | flops 33292288 | bytes 2097152 | tf_op jit(solution)/shard_map/reduce-window.8
  389.2 9.2 %fusion.108 = f32[4,256,2,128]{1,2,3,0:T(2,128)S(1)} fusion(f32[4,256,2,128]{1,3,2,0:T(8,128)S(1)} %bitcast.196), kind=kOutput, calls=%fused_computation.14.clone.1 | output fusion | flops 33292288 | bytes 2097152 | tf_op jit(solution)/shard_map/reduce-window.8
  401.9 2.4 fusion.68
  404.3 38.9 %all-gather.30.cloned.1.call-done = bf16[2048,512]{1,0:T(8,128)(2,1)} async-done(((bf16[128,512]{1,0:T(8,128)(2,1)}), bf16[2048,512]{1,0:T(8,128)(2,1)}) %all-gather.30.cloned.1.call-update) | async-done | bytes 2097168 | tf_op jit(solution)/shard_map/all_gather | solution.py:147
  443.2 3.3 fusion.31
  447.2 18.6 %reduce-scatter.2.cloned.1.call-done = bf16[128,2048]{1,0:T(8,128)(2,1)} async-done(((bf16[256,2048]{1,0:T(8,128)(2,1)}), bf16[128,2048]{1,0:T(8,128)(2,1)}) %reduce-scatter.2.cloned.1.call-update) | async-done | bytes 524304 | tf_op jit(solution)/shard_map/reduce_scatter | solution.py:218
  (181 shorter events, 43.2 us)
Async XLA Ops:
  7.2 47.2 %all-gather.16.cloned.1.call-start = ((), (), s32[]{:S(2)}) async-start(), calls=%async_computation.3 | async-start | bytes 2228224 | tf_op jit(solution)/shard_map/all_gather | solution.py:132
  7.9 88.8 %all-gather.12.cloned.1.call-start = ((), (), s32[]{:S(2)}) async-start(), calls=%async_computation.1 | async-start | bytes 2228224 | tf_op jit(solution)/shard_map/all_gather | solution.py:133
  8.6 130.4 %all-gather.22.cloned.1.call-start = ((), (), s32[]{:S(2)}) async-start(), calls=%async_computation.6 | async-start | bytes 2228224 | tf_op jit(solution)/shard_map/all_gather | solution.py:135
  9.4 171.9 %all-gather.26.cloned.1.call-start = ((), (), s32[]{:S(2)}) async-start(), calls=%async_computation.8 | async-start | bytes 2228224 | tf_op jit(solution)/shard_map/all_gather | solution.py:134
  10.0 213.6 %all-gather.24.cloned.1.call-start = ((), (), s32[]{:S(2)}) async-start(), calls=%async_computation.7 | async-start | bytes 2228224 | tf_op jit(solution)/shard_map/all_gather | solution.py:136
  10.5 284.0 %all-gather.28.cloned.1.call-start = ((), (), s32[]{:S(2)}) async-start(), calls=%async_computation.9 | async-start | bytes 2228224 | tf_op jit(solution)/shard_map/all_gather | solution.py:137
  11.1 300.8 %all-gather.14.cloned.1.call-start = ((), (), s32[]{:S(2)}) async-start(), calls=%async_computation.2 | async-start | bytes 2228224 | tf_op jit(solution)/shard_map/all_gather | solution.py:131
  11.9 346.6 %all-gather.18.cloned.1.call-start = ((), (), s32[]{:S(2)}) async-start(), calls=%async_computation.4 | async-start | bytes 2621440 | tf_op jit(solution)/shard_map/all_gather | solution.py:161
  13.4 83.3 %copy-start.4 = (bf16[1,256,2048]{2,1,0:T(8,128)(2,1)S(1)}, bf16[1,256,2048]{2,1,0:T(8,128)(2,1)}, u32[]{:S(2)}) copy-start(bf16[1,256,2048]{2,1,0:T(8,128)(2,1)} %param.23) | copy-start | bytes 3145732
  13.5 83.3 %copy-start.14 = (f32[2048]{0:T(1024)S(1)}, f32[2048]{0:T(1024)}, u32[]{:S(2)}) copy-start(f32[2048]{0:T(1024)} %param.24) | copy-start | bytes 24580
  57.0 0.7 copy-start.9
  99.1 3.1 copy-start.13
  99.1 40.0 %copy-start.15 = (f32[512]{0:T(512)S(1)}, f32[512]{0:T(512)}, u32[]{:S(2)}) copy-start(f32[512]{0:T(512)} %param.38) | copy-start | bytes 6148
  100.1 301.8 %all-gather.20.cloned.1.call-start = ((), (), s32[]{:S(2)}) async-start(), calls=%async_computation.5 | async-start | bytes 2228224 | tf_op jit(solution)/shard_map/all_gather | solution.py:146
  100.8 342.4 %all-gather.30.cloned.1.call-start = ((), (), s32[]{:S(2)}) async-start(), calls=%async_computation.10 | async-start | bytes 2228224 | tf_op jit(solution)/shard_map/all_gather | solution.py:147
  101.4 364.4 %reduce-scatter.2.cloned.1.call-start = ((), (), s32[]{:S(2)}) async-start(), calls=%async_computation.11 | async-start | bytes 1572864 | tf_op jit(solution)/shard_map/reduce_scatter | solution.py:218
  184.1 39.4 %copy-start.2 = (f32[256,512]{1,0:T(8,128)}, f32[256,512]{1,0:T(8,128)S(1)}, u32[]{:S(2)}) copy-start(f32[256,512]{1,0:T(8,128)S(1)} %divide_multiply_fusion) | copy-start | bytes 1572868
  250.5 41.5 %copy-start.8 = (f32[4,64,4,128]{3,1,0,2:T(8,128)S(1)}, f32[4,64,4,128]{3,1,0,2:T(8,128)}, u32[]{:S(2)}) copy-start(f32[4,64,4,128]{3,1,0,2:T(8,128)} %get-tuple-element.260) | copy-start | bytes 1572868
  279.8 12.4 %copy-start = (f32[256,4,128]{2,0,1:T(8,128)S(1)}, f32[256,4,128]{2,0,1:T(8,128)}, u32[]{:S(2)}) copy-start(f32[256,4,128]{2,0,1:T(8,128)} %copy_bitcast_fusion.3) | copy-start | bytes 1572868
  292.0 1.0 copy-start.3
  292.8 1.8 copy-start.5
  297.3 17.8 %copy-start.10 = (bf16[256,512]{1,0:T(8,128)(2,1)S(1)}, bf16[256,512]{1,0:T(8,128)(2,1)}, u32[]{:S(2)}) copy-start(bf16[256,512]{1,0:T(8,128)(2,1)} %copy-done.9) | copy-start | bytes 786436
  297.3 17.7 %copy-start.16 = (f32[4]{0:T(128)S(1)}, f32[4]{0:T(128)}, u32[]{:S(2)}) copy-start(f32[4]{0:T(128)} %param.34) | copy-start | bytes 52
  314.3 1.1 copy-start.7
  325.9 1.7 copy-start.1
  325.9 1.7 copy-start.11
  358.5 43.2 %copy-start.12 = (f32[512]{0:T(512)S(1)}, f32[512]{0:T(512)}, u32[]{:S(2)}) copy-start(f32[512]{0:T(512)} %param.35) | copy-start | bytes 6148
  401.9 41.3 %copy-start.6 = (bf16[256,4,128]{0,2,1:T(8,128)(2,1)S(1)}, bf16[256,4,128]{0,2,1:T(8,128)(2,1)}, u32[]{:S(2)}) copy-start(bf16[256,4,128]{0,2,1:T(8,128)(2,1)} %multiply_convert_fusion) | copy-start | bytes 786436
Sparse Core Ops, SparseCore 0:
  10.1 44.1 all-gather.15
  56.5 40.1 all-gather.11
  98.9 40.1 all-gather.21
  141.1 40.1 all-gather.25
  183.3 40.1 all-gather.23
  225.5 43.2 all-gather.27
  271.0 40.8 all-gather.13
  314.1 44.3 all-gather.17
  360.6 40.3 all-gather.19
  403.0 40.1 all-gather.29
  446.7 19.0 reduce-scatter.1
where the time goes:
time: 480 us; the launch traced here: 473 us
  waiting for transfers between devices  301 us (63%)
  other arithmetic  66.7 us (14%)
  matrix products  43.6 us (9%)
  blocking collectives  29.3 us (6%)
  between operations  14.7 us (3%)
  loops' own time  11.9 us (2%)
    all_gather x1, waiting for transfers between devices, on_device(): lax.all_gather(weights_in[1], ('sp', 'fs'), axis=0, tiled=True)  40.9 us
    all_gather x1, waiting for transfers between devices, on_device(): lax.all_gather(weights_in[5], ('sp', 'fs'), axis=0, tiled=True)  39.2 us
    all_gather x1, waiting for transfers between devices, on_device(): lax.all_gather(emitted_projection_linear_scan, ('sp', 'fs'), axis=0, tile...  38.9 us
    all_gather x1, waiting for transfers between devices, on_device(): lax.all_gather(weights_in[2], ('sp', 'fs'), axis=0, tiled=True)  38.9 us
    all_gather x1, waiting for transfers between devices, on_device(): lax.all_gather(weights_in[3], ('sp', 'fs'), axis=0, tiled=True)  37.7 us
    another operation x10, other arithmetic  37.4 us
    all_gather x1, waiting for transfers between devices, on_device(): lax.all_gather(weights_in[4], ('sp', 'fs'), axis=0, tiled=True)  36.9 us
    all_gather x1, waiting for transfers between devices, on_device(): gathered = lax.all_gather(key_value, 'sp', axis=1, tiled=True)  29.9 us
  transfers between devices with their start and end apart: 11, of which 9 were waited for; matrix products, arithmetic and copies ran while one was open for 23% of the time, Pallas kernels for 0%

commit v1 on v0

--- a/solution.py
+++ b/solution.py
@@ -1,6 +1,9 @@
+import functools
 import jax
 import jax.numpy as jnp
 from jax import lax
+from jax.experimental import pallas as pl
+from jax.experimental.pallas import tpu as pltpu
 from jax.sharding import PartitionSpec as P
 
 HEAD = 128
@@ -95,7 +98,7 @@
     )
 
 
-def on_device(
+def on_device_general(
     input_layer_rows,
     input_norm_gain,
     query_weight_attention,
@@ -225,7 +228,446 @@
     return (layer_out, row_log_total)
 
 
+LEAF = 16
+CHUNK = 128
+TILE = 256
+MESH = pl.DeviceIdType.MESH
+
+
+def remote(src, dst, send, recv, **where):
+    return pltpu.make_async_remote_copy(
+        src_ref=src, dst_ref=dst, send_sem=send, recv_sem=recv, device_id=where, device_id_type=MESH
+    )
+
+
+def greet(peers):
+    barrier = pltpu.get_barrier_semaphore()
+    for where in peers:
+        pl.semaphore_signal(barrier, inc=1, device_id=where, device_id_type=MESH)
+    pl.semaphore_wait(barrier, len(peers))
+
+
+def gather_kernel(
+    n, x_ref, w_ref, e_ref, o_ref, X, W, E, O,
+    x_send, x_recv, xx_send, xx_recv,
+    w_send, w_recv, wy_send, wy_recv, wc_send, wc_recv, wd_send, wd_recv,
+    e_send, e_recv,
+    o_send, o_recv, oy_send, oy_recv, oc_send, oc_recv, od_send, od_recv,
+    local_sem,
+):
+    z, f, x = lax.axis_index("sp"), lax.axis_index("fs"), lax.axis_index("tp")
+    core, row, side = f + 1 - 2 * (f % 2), (f + 2) % 4, 1 - x
+    half = x_ref.shape[0] // 2
+    mine = pl.ds(pl.multiple_of(x * half, half), half)
+    greet(
+        [{"sp": (z + o) % n} for o in range(1, n)] + [{"fs": core}, {"fs": row}, {"tp": side}]
+    )
+
+    def reach(direction, k):
+        if direction == 0:
+            return (z - k >= 0) & (z + 1 < n), z - 1 - k >= 0, z - k, z - 1 - k, z + 1
+        return (z + k < n) & (z - 1 >= 0), z + 1 + k < n, z + k, z + 1 + k, z - 1
+
+    def x_copy(direction, k):
+        _, _, out, _, to = reach(direction, k)
+        src = x_ref.at[mine] if k == 0 else X.at[out, mine]
+        return remote(src, X.at[out, mine], x_send.at[direction, k], x_recv.at[direction, k], sp=to)
+
+    def xx_copy(direction, k):
+        block = reach(direction, k)[3]
+        return remote(X.at[block, mine], X.at[block, mine], xx_send.at[direction, k], xx_recv.at[direction, k], tp=side)
+
+    def o_copy(direction, k):
+        _, _, out, _, to = reach(direction, k)
+        src = o_ref if k == 0 else O.at[out, f]
+        return remote(src, O.at[out, f], o_send.at[direction, k], o_recv.at[direction, k], sp=to)
+
+    def o_side(kind, direction, k):
+        block = reach(direction, k)[3]
+        if kind == 0:
+            return remote(O.at[block, f], O.at[block, f], oy_send.at[direction, k], oy_recv.at[direction, k], fs=row)
+        if kind == 1:
+            return remote(O.at[block, f], O.at[block, f], oc_send.at[direction, k], oc_recv.at[direction, k], fs=core)
+        return remote(O.at[block, row], O.at[block, row], od_send.at[direction, k], od_recv.at[direction, k], fs=core)
+
+    def o_own(kind):
+        if kind == 0:
+            return remote(o_ref, O.at[z, f], oy_send.at[2, 0], oy_recv.at[2, 0], fs=row)
+        if kind == 1:
+            return remote(o_ref, O.at[z, f], oc_send.at[2, 0], oc_recv.at[2, 0], fs=core)
+        return remote(O.at[z, row], O.at[z, row], od_send.at[2, 0], od_recv.at[2, 0], fs=core)
+
+    def w_copy(o):
+        return remote(w_ref.at[(z + o) % n], W.at[z, f], w_send.at[o], w_recv.at[o], sp=(z + o) % n)
+
+    def e_copy(o):
+        return remote(e_ref.at[(z + o) % n], E.at[z], e_send.at[o], e_recv.at[o], sp=(z + o) % n)
+
+    def w_side(kind, o):
+        block = (z - o + n) % n
+        src = w_ref.at[z] if o == 0 else W.at[block, f]
+        if kind == 0:
+            return remote(src, W.at[block, f], wy_send.at[o], wy_recv.at[o], fs=row)
+        if kind == 1:
+            return remote(src, W.at[block, f], wc_send.at[o], wc_recv.at[o], fs=core)
+        return remote(W.at[block, row], W.at[block, row], wd_send.at[o], wd_recv.at[o], fs=core)
+
+    def sends(copy, direction, k):
+        @pl.when(reach(direction, k)[0])
+        def _():
+            copy(direction, k).start()
+
+    def received(direction, k, act):
+        pl.when(reach(direction, k)[1])(act)
+
+    both = (0, 1)
+    for d in both:
+        sends(x_copy, d, 0)
+    local = [
+        pltpu.make_async_copy(x_ref, X.at[z], local_sem.at[0]),
+        pltpu.make_async_copy(w_ref.at[z], W.at[z, f], local_sem.at[1]),
+        pltpu.make_async_copy(e_ref.at[z], E.at[z], local_sem.at[2]),
+        pltpu.make_async_copy(o_ref, O.at[z, f], local_sem.at[3]),
+    ]
+    for copy in local:
+        copy.start()
+    for kind in both:
+        w_side(kind, 0).start()
+    for o in range(1, n):
+        w_copy(o).start()
+    for o in range(1, n):
+        e_copy(o).start()
+    for d in both:
+        sends(o_copy, d, 0)
+    for kind in both:
+        o_own(kind).start()
+    for k in range(n - 1):
+        for d in both:
+            def x_here(d=d, k=k):
+                x_copy(d, k).wait_recv()
+                xx_copy(d, k).start()
+            received(d, k, x_here)
+            if k + 1 < n - 1:
+                sends(x_copy, d, k + 1)
+        w_copy(k + 1).wait_recv()
+        for kind in both:
+            w_side(kind, k + 1).start()
+        for d in both:
+            def o_here(d=d, k=k):
+                o_copy(d, k).wait_recv()
+                for kind in both:
+                    o_side(kind, d, k).start()
+            received(d, k, o_here)
+            if k + 1 < n - 1:
+                sends(o_copy, d, k + 1)
+    for o in range(n):
+        w_side(0, o).wait_recv()
+        w_side(2, o).start()
+    o_own(0).wait_recv()
+    o_own(2).start()
+    for k in range(n - 1):
+        for d in both:
+            def o_next(d=d, k=k):
+                o_side(0, d, k).wait_recv()
+                o_side(2, d, k).start()
+            received(d, k, o_next)
+    for o in range(n):
+        w_side(1, o).wait_recv()
+        w_side(2, o).wait_recv()
+        for kind in range(3):
+            w_side(kind, o).wait_send()
+    for o in range(1, n):
+        e_copy(o).wait_recv()
+        e_copy(o).wait_send()
+        w_copy(o).wait_send()
+    o_own(1).wait_recv()
+    o_own(2).wait_recv()
+    for kind in range(3):
+        o_own(kind).wait_send()
+    for k in range(n - 1):
+        for d in both:
+            def rest(d=d, k=k):
+                xx_copy(d, k).wait_recv()
+                xx_copy(d, k).wait_send()
+                o_side(1, d, k).wait_recv()
+                o_side(2, d, k).wait_recv()
+                for kind in range(3):
+                    o_side(kind, d, k).wait_send()
+            received(d, k, rest)
+
+            @pl.when(reach(d, k)[0])
+            def _(d=d, k=k):
+                x_copy(d, k).wait_send()
+                o_copy(d, k).wait_send()
+    for copy in local:
+        copy.wait()
+
+
+def nt_dot(a, b):
+    return lax.dot_general(a, b, (((1,), (1,)), ((), ())), preferred_element_type=jnp.float32)
+
+
+def tn_dot(a, b):
+    return lax.dot_general(a, b, (((0,), (0,)), ((), ())), preferred_element_type=jnp.float32)
+
+
+def grid_of(shape):
+    return lax.broadcasted_iota(jnp.int32, shape, 0), lax.broadcasted_iota(jnp.int32, shape, 1)
+
+
+def mixer_kernel(p_ref, e_ref, shift_ref, again_ref, rgain_ref, floor_ref, foff_ref, m_ref, keep_ref):
+    rows = p_ref.shape[0]
+    shift = shift_ref[...]
+    r, c = grid_of((TILE, TILE))
+    later = (r > c).astype(jnp.bfloat16)
+    for i in range(rows // TILE):
+        here = slice(i * TILE, (i + 1) * TILE)
+        query = p_ref[here, 0:HEAD]
+        total = jnp.zeros((TILE, HEAD), jnp.float32)
+        keep = jnp.zeros((TILE, 1), jnp.float32)
+        for j in range(i, -1, -1):
+            there = slice(j * TILE, (j + 1) * TILE)
+            score = nt_dot(query, p_ref[there, HEAD : 2 * HEAD]) * HEAD ** (-0.5) + shift
+            soft = -(jnp.maximum(score, 0.0) + jnp.log1p(jnp.exp(-jnp.abs(score))))
+            held = jnp.where(r > c, soft, 0.0) if i == j else soft
+            high = held.astype(jnp.bfloat16)
+            low = (held - high.astype(jnp.float32)).astype(jnp.bfloat16)
+            suffix = jnp.dot(high, later, preferred_element_type=jnp.float32) + jnp.dot(
+                low, later, preferred_element_type=jnp.float32
+            )
+            weight = jnp.exp(score + soft + suffix + keep)
+            if i == j:
+                weight = jnp.where(r > c, weight, 0.0)
+            total += jnp.dot(
+                weight.astype(jnp.bfloat16),
+                p_ref[there, 2 * HEAD : 3 * HEAD],
+                preferred_element_type=jnp.float32,
+            )
+            keep += jnp.sum(held, axis=1, keepdims=True)
+        m_ref[here, 0:HEAD] = head_norm(total, again_ref[...]).astype(jnp.bfloat16)
+        keep_ref[here, :] = keep
+
+    floor, offset, gain = floor_ref[...], foff_ref[...], rgain_ref[...]
+    r, c = grid_of((CHUNK, CHUNK))
+    lower = (r >= c).astype(jnp.float32)
+
+    def chunk(i, state):
+        here = pl.ds(pl.multiple_of(i * CHUNK, CHUNK), CHUNK)
+        part = lambda k: p_ref[here, k * HEAD : (k + 1) * HEAD].astype(jnp.float32)
+        raw = part(3)
+        query = raw * jax.nn.sigmoid(raw)
+        key = (1.0 - floor) * jax.nn.sigmoid(-(part(4) + offset))
+        value = p_ref[here, 5 * HEAD : 6 * HEAD]
+        gate = part(6)
+        decay = jnp.log1p(-key) + e_ref[here, :].astype(jnp.float32)
+        run = jnp.dot(lower, decay, precision=lax.Precision.HIGHEST, preferred_element_type=jnp.float32)
+        stripes = [jnp.zeros((LEAF, CHUNK), jnp.float32)]
+        for s in range(LEAF, CHUNK, LEAF):
+            edge = run[s - 1 : s, :]
+            near = (query[s : s + LEAF] * jnp.exp(run[s : s + LEAF] - edge)).astype(jnp.bfloat16)
+            far = (key * jnp.exp(jnp.where(r < s, edge - run, -jnp.inf))).astype(jnp.bfloat16)
+            stripes.append(nt_dot(near, far))
+        pairs = jnp.concatenate(stripes, axis=0)
+        for d in range(LEAF):
+            back_key = pltpu.roll(key, d, 0) if d else key
+            back_run = pltpu.roll(run, d, 0) if d else run
+            gap = jnp.where(r % LEAF >= d, run - back_run, -jnp.inf)
+            column = jnp.sum(query * back_key * jnp.exp(gap), axis=1, keepdims=True)
+            pairs = jnp.where((r - c == d) & (r % LEAF >= d), column, pairs)
+        last = run[CHUNK - 1 : CHUNK, :]
+        out = jnp.dot(pairs.astype(jnp.bfloat16), value, preferred_element_type=jnp.float32)
+        out += nt_dot((query * jnp.exp(run)).astype(jnp.bfloat16), state.astype(jnp.bfloat16))
+        mixed = head_norm(out, gain) * (gate * jax.nn.sigmoid(gate))
+        m_ref[here, HEAD : 2 * HEAD] = mixed.astype(jnp.bfloat16)
+        return jnp.exp(last) * state + tn_dot(value, (key * jnp.exp(last - run)).astype(jnp.bfloat16))
+
+    lax.fori_loop(0, rows // CHUNK, chunk, jnp.zeros((HEAD, HEAD), jnp.float32))
+
+
+PIECES = 4
+
+
+def output_kernel(
+    n, m_ref, t_ref, o_ref, out_ref, T, M, away, landed,
+    m_send, m_recv, t_send, t_recv, y_send, y_recv, local_sem,
+):
+    z, x = lax.axis_index("sp"), lax.axis_index("tp")
+    side = 1 - x
+    half = out_ref.shape[0]
+    greet([{"sp": (z + o) % n} for o in range(1, n)] + [{"tp": side}])
+
+    def m_copy(o):
+        return remote(m_ref.at[(z + o) % n], M.at[z], m_send.at[o], m_recv.at[o], sp=(z + o) % n)
+
+    def t_copy(o):
+        return remote(t_ref.at[(z + o) % n], T.at[z], t_send.at[o], t_recv.at[o], sp=(z + o) % n)
+
+    for o in range(1, n):
+        m_copy(o).start()
+    for o in range(1, n):
+        t_copy(o).start()
+    local = [
+        pltpu.make_async_copy(m_ref.at[z], M.at[z], local_sem.at[0]),
+        pltpu.make_async_copy(t_ref.at[z], T.at[z], local_sem.at[1]),
+    ]
+    for copy in local:
+        copy.start()
+    for copy in local:
+        copy.wait()
+    for o in range(1, n):
+        m_copy(o).wait()
+
+    def rows_of(which):
+        rows = pl.ds(pl.multiple_of(which * half, half), half)
+        parts = [M[k, rows, g * HEAD : (g + 1) * HEAD] for g in (0, 1) for k in range(n)]
+        return jnp.concatenate(parts, axis=1)
+
+    width = out_ref.shape[1] // PIECES
+
+    def y_copy(j):
+        return remote(away.at[j], landed.at[j], y_send.at[j], y_recv.at[j], tp=side)
+
+    theirs = rows_of(side)
+    for j in range(PIECES):
+        away[j] = nt_dot(theirs, o_ref[j * width : (j + 1) * width, :]).astype(jnp.bfloat16)
+        if j:
+            y_copy(j - 1).start()
+    ours = rows_of(x)
+    for j in range(PIECES):
+        piece = nt_dot(ours, o_ref[j * width : (j + 1) * width, :])
+        if j == 0:
+            y_copy(PIECES - 1).start()
+        y_copy(j).wait_recv()
+        piece += landed[j].astype(jnp.float32)
+        out_ref[:, j * width : (j + 1) * width] = piece.astype(jnp.bfloat16)
+    for j in range(PIECES):
+        y_copy(j).wait_send()
+    for o in range(1, n):
+        t_copy(o).wait()
+
+
+VMEM = pl.BlockSpec(memory_space=pltpu.VMEM)
+DMA = pltpu.SemaphoreType.DMA
+
+
+def on_device_heads(
+    n,
+    input_layer_rows,
+    input_norm_gain,
+    query_weight_attention,
+    key_weight_attention,
+    value_weight_attention,
+    query_weight_recurrent,
+    forget_weight_recurrent,
+    value_weight_recurrent,
+    gate_weight_recurrent,
+    output_weight_attention,
+    emitted_projection_linear_scan,
+    score_offset,
+    attention_norm_gain,
+    recurrence_norm_gain,
+    forget_floor,
+    forget_offset,
+    extra_log_decay,
+):
+    values = input_layer_rows[0].astype(jnp.float32)
+    square_mean = jnp.mean(values * values, axis=-1, keepdims=True)
+    normed = (values * lax.rsqrt(square_mean + epsilon) * input_norm_gain).astype(jnp.bfloat16)
+    tokens, depth = normed.shape
+    groups = lax.axis_size("fs")
+    weights_in = (
+        query_weight_attention,
+        key_weight_attention,
+        value_weight_attention,
+        query_weight_recurrent,
+        forget_weight_recurrent,
+        value_weight_recurrent,
+        gate_weight_recurrent,
+    )
+    share = weights_in[0].shape[0]
+    width = len(weights_in) * HEAD
+    by_head = jnp.stack(
+        [
+            jnp.concatenate([w[:, h * HEAD : (h + 1) * HEAD] for w in weights_in], axis=1)
+            for h in range(n)
+        ]
+    )
+    extra = extra_log_decay[0].astype(jnp.bfloat16)
+    extra = jnp.stack([extra[:, h * HEAD : (h + 1) * HEAD] for h in range(n)])
+    both_out = jnp.concatenate([output_weight_attention, emitted_projection_linear_scan], axis=1)
+    X, W, E, O = pl.pallas_call(
+        functools.partial(gather_kernel, n),
+        out_shape=(
+            jax.ShapeDtypeStruct((n, tokens, depth), jnp.bfloat16),
+            jax.ShapeDtypeStruct((n, groups, share, width), jnp.bfloat16),
+            jax.ShapeDtypeStruct((n, tokens, HEAD), jnp.bfloat16),
+            jax.ShapeDtypeStruct((n, groups, share, both_out.shape[1]), jnp.bfloat16),
+        ),
+        in_specs=[VMEM] * 4,
+        out_specs=(VMEM,) * 4,
+        scratch_shapes=[DMA((2, n))] * 4 + [DMA((n,))] * 10 + [DMA((2, n))] * 2 + [DMA((3, n))] * 6 + [DMA((4,))],
+        compiler_params=pltpu.CompilerParams(
+            collective_id=0, has_side_effects=True, vmem_limit_bytes=50 * 1024 * 1024
+        ),
+    )(normed, by_head, extra, both_out)
+    projected = jnp.dot(
+        X.reshape(n * tokens, depth), W.reshape(depth, width), preferred_element_type=jnp.float32
+    ).astype(jnp.bfloat16)
+    z = lax.axis_index("sp")
+    own = lambda a: lax.dynamic_slice_in_dim(a, z * HEAD, HEAD)[None]
+    mixed, keep = pl.pallas_call(
+        mixer_kernel,
+        out_shape=(
+            jax.ShapeDtypeStruct((n * tokens, 2 * HEAD), jnp.bfloat16),
+            jax.ShapeDtypeStruct((n * tokens, 1), jnp.float32),
+        ),
+        in_specs=[VMEM] * 7,
+        out_specs=(VMEM,) * 2,
+        compiler_params=pltpu.CompilerParams(vmem_limit_bytes=40 * 1024 * 1024),
+    )(
+        projected,
+        E.reshape(n * tokens, HEAD),
+        lax.dynamic_slice_in_dim(score_offset, z, 1)[None],
+        own(attention_norm_gain),
+        own(recurrence_norm_gain),
+        own(forget_floor),
+        own(forget_offset),
+    )
+    totals = jnp.log(jnp.maximum(-jnp.expm1(keep[:, 0]), log_floor)).reshape(n, 1, tokens)
+    totals = jnp.broadcast_to(totals, (n, 8, tokens))
+    half = tokens // 2
+    layer_out, T = pl.pallas_call(
+        functools.partial(output_kernel, n),
+        out_shape=(
+            jax.ShapeDtypeStruct((half, depth), jnp.bfloat16),
+            jax.ShapeDtypeStruct((n, 8, tokens), jnp.float32),
+        ),
+        in_specs=[VMEM] * 3,
+        out_specs=(VMEM,) * 2,
+        scratch_shapes=[
+            pltpu.VMEM((n, tokens, 2 * HEAD), jnp.bfloat16),
+            pltpu.VMEM((PIECES, half, depth // PIECES), jnp.bfloat16),
+            pltpu.VMEM((PIECES, half, depth // PIECES), jnp.bfloat16),
+        ]
+        + [DMA((n,))] * 4
+        + [DMA((PIECES,))] * 2
+        + [DMA((2,))],
+        compiler_params=pltpu.CompilerParams(
+            collective_id=1, has_side_effects=True, vmem_limit_bytes=40 * 1024 * 1024
+        ),
+    )(mixed.reshape(n, tokens, 2 * HEAD), totals, O.reshape(depth, both_out.shape[1]))
+    return (layer_out[None], T[:, 0, :][None])
+
+
 def solution(mesh):
+    n = mesh.shape["sp"]
+    heads_fit = mesh.shape["fs"] == 4 and mesh.shape["tp"] == 2 and n > 1
+
+    def on_device(*args):
+        if heads_fit and args[11].shape[0] == n and args[0].shape[1] % TILE == 0:
+            return on_device_heads(n, *args)
+        return on_device_general(*args)
+
     return jax.shard_map(
         on_device,
         mesh=mesh,

time: 480 us -> 153 us (0.32); the launches traced: 473 us -> 152 us
  waiting for transfers between devices: 301 us -> 0 us
  Pallas kernels: 0 us -> 130 us
  other arithmetic: 66.7 us -> 1.15 us
  matrix products: 43.6 us -> 7.8 us
  blocking collectives: 29.3 us -> 0 us
  between operations: 14.7 us -> 0.85 us
  loops' own time: 11.9 us -> 0 us
  local copies, waits for them, and re-layouts: 4.66 us -> 11.9 us
    all_gather x10 -> x0, waiting for transfers between devices: 277 us -> none  [the longest x1 40.9 us: on_device(): lax.all_gather(weights_in[1], ('sp', 'fs'), axis=0, tiled=True)]
    pallas_call x0 -> x3, Pallas kernels: none -> 130 us  [the longest x1 91.4 us: on_device_heads(): pl.pallas_call(functools.partial(gather_kernel, n), out_shape=(jax.ShapeD...]
    another operation x19 -> x2, other arithmetic: 40 us -> 0.18 us  [the longest x1 0.14 us: on_device_heads(): jnp.stack([jnp.concatenate([w[:, h * HEAD:(h + 1) * HEAD] for w in weight...]
    dot_general x30 -> x1, matrix products: 43.6 us -> 7.8 us  [on_device_heads(): jnp.dot(X.reshape(n * tokens, depth), W.reshape(depth, width), preferred_...]
    all_gather x2 -> x0, blocking collectives: 29.3 us -> none  [entering(): lax.all_gather(part.astype(kind), axis)]
    reduce_scatter x1 -> x0, waiting for transfers between devices: 18.6 us -> none  [on_device(): lax.psum_scatter((contract_rows(mixed_a, out_a) + contract_rows(mixed_b,...]
    reduce_sum x7 -> x1, other arithmetic: 17.2 us -> 0.29 us  [on_device_heads(): square_mean = jnp.mean(values * values, axis=-1, keepdims=True)]
    another operation x3 -> x0, loops' own time: 11.9 us -> none  [the longest x1 11.4 us: entering(): return lax.fori_loop(0, size, hop, start)]
  transfers between devices with their start and end apart: 11 -> 0, of which waited for: 9 -> 0; matrix products, arithmetic and copies ran while one was open for 23% -> 0% of each run, Pallas kernels for 0% -> 0%
where the time goes in v1:
time: 153 us; the launch traced here: 152 us
  Pallas kernels  130 us (85%)
  local copies, waits for them, and re-layouts  11.9 us (8%)
  matrix products  7.8 us (5%)
    pallas_call x1, Pallas kernels, on_device_heads(): pl.pallas_call(functools.partial(gather_kernel, n), out_shape=(jax.ShapeD...  91.4 us
    pallas_call x1, Pallas kernels, on_device_heads(): pl.pallas_call(functools.partial(output_kernel, n), out_shape=(jax.ShapeD...  27 us
    pallas_call x1, Pallas kernels, on_device_heads(): pl.pallas_call(mixer_kernel, out_shape=(jax.ShapeDtypeStruct((n * tokens,...  11.7 us
    unnamed x22, local copies, waits for them, and re-layouts  8.82 us
    dot_general x1, matrix products, on_device_heads(): jnp.dot(X.reshape(n * tokens, depth), W.reshape(depth, width), preferred_...  7.8 us

profile of v1, /device:TPU:0, one launch (start us, length us, event | category | flops | bytes accessed | tf_op | source)
XLA Modules:
  0.0 151.8 jit_solution(13344517634907133621)
XLA Ops:
  0.6 0.0 copy-start.2
  0.6 0.0 copy-start.1
  0.7 0.0 copy-start.5
  0.7 0.9 constant_dynamic-update-slice_fusion.6
  1.6 0.8 constant_dynamic-update-slice_fusion.5
  2.5 0.8 constant_dynamic-update-slice_fusion.4
  3.3 0.8 constant_dynamic-update-slice_fusion.3
  4.2 0.8 constant_dynamic-update-slice_fusion.2
  5.0 0.0 copy-start.3
  5.0 0.0 copy-start.4
  5.0 0.9 constant_dynamic-update-slice_fusion.1
  5.9 0.8 constant_dynamic-update-slice_fusion
  6.8 0.1 pad_maximum_fusion.w_ref
  6.9 0.0 copy-done.2
  7.1 0.0 copy-done.1
  7.1 0.3 fusion
  7.4 0.3 fusion.2.x_ref
  7.7 0.0 copy-done.3
  7.7 0.0 copy-done.4
  7.8 91.4 %shard_map.176 = (bf16[4,256,2048]{2,1,0:T(8,128)(2,1)}, bf16[4,4,128,896]{3,2,1,0:T(8,128)(2,1)}, bf16[4,256,128]{2,1,0:T(8,128)(2,1)S(1)}, bf16[4,4,128,1024]{3,2,1,0:T(8,128)(2,1)}) custom-call(bf16[256,2048]{1,0:T(8,128)(2,1)S(1)} %fusion.2.x_ref, bf16[4,128,896]{2,1,0:T(8,128)(2,1)S(1)} %pad_maximum_fusion.w_ref, ...), custom_call_target="tpu_custom_call" | custom-call | tf_op jit(solution)/shard_map/pallas_call | solution.py:598
  99.2 0.0 copy-start.6
  99.2 7.8 %convolution_convert_fusion.p_ref = bf16[1024,896]{1,0:T(8,128)(2,1)S(1)} fusion(bf16[1024,2048]{1,0:T(8,128)(2,1)} %bitcast.45, bf16[2048,896]{1,0:T(8,128)(2,1)} %bitcast.46), kind=kOutput, calls=%fused_computation.5 | convolution fusion | flops 3759013888 | bytes 9699328 | tf_op jit(solution)/shard_map/dot_general | solution.py:613
  107.0 0.8 dynamic-slice_bitcast_fusion
  107.8 0.8 dynamic-slice_bitcast_fusion.2
  108.6 0.6 dynamic_slice.15
  109.2 11.7 %shard_map.177 = (bf16[1024,256]{1,0:T(8,128)(2,1)S(1)}, f32[1024,1]{1,0:T(8,128)S(1)}) custom-call(bf16[1024,896]{1,0:T(8,128)(2,1)S(1)} %convolution_convert_fusion.p_ref, bf16[1024,128]{1,0:T(8,128)(2,1)S(1)} %bitcast.40, f32[1,1]{1,0:T(1,128)} %bitcast.14.shift_ref, f32[1,128]{1,0:T(1,128)S(1)} %get-tuple-element.57.again_ref, ...), custom_call_target="tpu_custom_call" | custom-call | tf_op jit(solution)/shard_map/pallas_call | solution.py:618
  120.8 0.3 log_reduce_fusion
  121.2 0.0 copy-start
  121.2 2.2 %copy-done = bf16[4,4,128,1024]{3,2,1,0:T(8,128)(2,1)S(1)} copy-done((bf16[4,4,128,1024]{3,2,1,0:T(8,128)(2,1)S(1)}, bf16[4,4,128,1024]{3,2,1,0:T(8,128)(2,1)}, u32[]{:S(2)}) %copy-start) | copy-done | bytes 4194328
  123.4 27.0 %shard_map.178 = (bf16[128,2048]{1,0:T(8,128)(2,1)S(1)}, f32[4,8,256]{2,1,0:T(8,128)S(1)}) custom-call(bf16[4,256,256]{2,1,0:T(8,128)(2,1)S(1)} %bitcast.38, f32[4,8,256]{2,1,0:T(8,128)S(1)} %broadcast_in_dim.30.t_ref, bf16[2048,1024]{1,0:T(8,128)(2,1)S(1)} %bitcast.37), custom_call_target="tpu_custom_call" | custom-call | tf_op jit(solution)/shard_map/pallas_call | solution.py:639
  150.4 0.6 copy.20
  151.0 0.8 copy.46
  (10 shorter events, 0.2 us)
Async XLA Ops:
  0.6 6.3 %copy-start.2 = (f32[1,256,512]{2,1,0:T(8,128)S(1)}, f32[1,256,512]{2,1,0:T(8,128)}, u32[]{:S(2)}) copy-start(f32[1,256,512]{2,1,0:T(8,128)} %param.33) | copy-start | bytes 1572868
  0.6 6.4 %copy-start.1 = (bf16[1,256,2048]{2,1,0:T(8,128)(2,1)S(1)}, bf16[1,256,2048]{2,1,0:T(8,128)(2,1)}, u32[]{:S(2)}) copy-start(bf16[1,256,2048]{2,1,0:T(8,128)(2,1)} %param.17) | copy-start | bytes 3145732
  0.7 6.7 %copy-start.5 = (f32[2048]{0:T(1024)S(1)}, f32[2048]{0:T(1024)}, u32[]{:S(2)}) copy-start(f32[2048]{0:T(1024)} %param.18) | copy-start | bytes 24580
  5.0 2.7 %copy-start.3 = (bf16[128,512]{1,0:T(8,128)(2,1)S(1)}, bf16[128,512]{1,0:T(8,128)(2,1)}, u32[]{:S(2)}) copy-start(bf16[128,512]{1,0:T(8,128)(2,1)} %param.27) | copy-start | bytes 393220
  5.0 2.7 %copy-start.4 = (bf16[128,512]{1,0:T(8,128)(2,1)S(1)}, bf16[128,512]{1,0:T(8,128)(2,1)}, u32[]{:S(2)}) copy-start(bf16[128,512]{1,0:T(8,128)(2,1)} %param.26) | copy-start | bytes 393220
  99.2 9.4 %copy-start.6 = (f32[4]{0:T(128)S(1)}, f32[4]{0:T(128)}, u32[]{:S(2)}) copy-start(f32[4]{0:T(128)} %param.28) | copy-start | bytes 52
  121.2 2.2 %copy-start = (bf16[4,4,128,1024]{3,2,1,0:T(8,128)(2,1)S(1)}, bf16[4,4,128,1024]{3,2,1,0:T(8,128)(2,1)}, u32[]{:S(2)}) copy-start(bf16[4,4,128,1024]{3,2,1,0:T(8,128)(2,1)} %get-tuple-element.15) | copy-start | bytes 12582916

commit v2 on v0

--- a/solution.py
+++ b/solution.py
@@ -1,6 +1,9 @@
+import functools
 import jax
 import jax.numpy as jnp
 from jax import lax
+from jax.experimental import pallas as pl
+from jax.experimental.pallas import tpu as pltpu
 from jax.sharding import PartitionSpec as P
 
 HEAD = 128
@@ -95,7 +98,7 @@
     )
 
 
-def on_device(
+def on_device_general(
     input_layer_rows,
     input_norm_gain,
     query_weight_attention,
@@ -225,7 +228,518 @@
     return (layer_out, row_log_total)
 
 
+LEAF = 16
+CHUNK = 128
+TILE = 256
+MESH = pl.DeviceIdType.MESH
+
+
+def remote(src, dst, send, recv, **where):
+    return pltpu.make_async_remote_copy(
+        src_ref=src, dst_ref=dst, send_sem=send, recv_sem=recv, device_id=where, device_id_type=MESH
+    )
+
+
+def greet(peers):
+    barrier = pltpu.get_barrier_semaphore()
+    for where in peers:
+        pl.semaphore_signal(barrier, inc=1, device_id=where, device_id_type=MESH)
+    pl.semaphore_wait(barrier, len(peers))
+
+
+def nt_dot(a, b):
+    return lax.dot_general(a, b, (((1,), (1,)), ((), ())), preferred_element_type=jnp.float32)
+
+
+def tn_dot(a, b):
+    return lax.dot_general(a, b, (((0,), (0,)), ((), ())), preferred_element_type=jnp.float32)
+
+
+def grid_of(shape):
+    return lax.broadcasted_iota(jnp.int32, shape, 0), lax.broadcasted_iota(jnp.int32, shape, 1)
+
+
+def attend_tile(i, p_ref, shift, gain):
+    here = slice(i * TILE, (i + 1) * TILE)
+    r, c = grid_of((TILE, TILE))
+    later = (r > c).astype(jnp.bfloat16)
+    query = p_ref[here, 0:HEAD]
+    total = jnp.zeros((TILE, HEAD), jnp.float32)
+    keep = jnp.zeros((TILE, 1), jnp.float32)
+    for j in range(i, -1, -1):
+        there = slice(j * TILE, (j + 1) * TILE)
+        score = nt_dot(query, p_ref[there, HEAD : 2 * HEAD]) * HEAD ** (-0.5) + shift
+        soft = -(jnp.maximum(score, 0.0) + jnp.log1p(jnp.exp(-jnp.abs(score))))
+        held = jnp.where(r > c, soft, 0.0) if i == j else soft
+        high = held.astype(jnp.bfloat16)
+        low = (held - high.astype(jnp.float32)).astype(jnp.bfloat16)
+        suffix = jnp.dot(high, later, preferred_element_type=jnp.float32) + jnp.dot(
+            low, later, preferred_element_type=jnp.float32
+        )
+        weight = jnp.exp(score + soft + suffix + keep)
+        if i == j:
+            weight = jnp.where(r > c, weight, 0.0)
+        total += jnp.dot(
+            weight.astype(jnp.bfloat16),
+            p_ref[there, 2 * HEAD : 3 * HEAD],
+            preferred_element_type=jnp.float32,
+        )
+        keep += jnp.sum(held, axis=1, keepdims=True)
+    return head_norm(total, gain).astype(jnp.bfloat16), keep
+
+
+def recur_chunk(p_ref, e_ref, here, state, floor, offset, gain):
+    r, c = grid_of((CHUNK, CHUNK))
+    lower = (r >= c).astype(jnp.float32)
+    part = lambda k: p_ref[here, k * HEAD : (k + 1) * HEAD].astype(jnp.float32)
+    raw = part(3)
+    query = raw * jax.nn.sigmoid(raw)
+    key = (1.0 - floor) * jax.nn.sigmoid(-(part(4) + offset))
+    value = p_ref[here, 5 * HEAD : 6 * HEAD]
+    gate = part(6)
+    decay = jnp.log1p(-key) + e_ref[...].astype(jnp.float32)
+    run = jnp.dot(lower, decay, precision=lax.Precision.HIGHEST, preferred_element_type=jnp.float32)
+    stripes = [jnp.zeros((LEAF, CHUNK), jnp.float32)]
+    for s in range(LEAF, CHUNK, LEAF):
+        edge = run[s - 1 : s, :]
+        near = (query[s : s + LEAF] * jnp.exp(run[s : s + LEAF] - edge)).astype(jnp.bfloat16)
+        far = (key * jnp.exp(jnp.where(r < s, edge - run, -jnp.inf))).astype(jnp.bfloat16)
+        stripes.append(nt_dot(near, far))
+    pairs = jnp.concatenate(stripes, axis=0)
+    for d in range(LEAF):
+        back_key = pltpu.roll(key, d, 0) if d else key
+        back_run = pltpu.roll(run, d, 0) if d else run
+        gap = jnp.where(r % LEAF >= d, run - back_run, -jnp.inf)
+        column = jnp.sum(query * back_key * jnp.exp(gap), axis=1, keepdims=True)
+        pairs = jnp.where((r - c == d) & (r % LEAF >= d), column, pairs)
+    last = run[CHUNK - 1 : CHUNK, :]
+    out = jnp.dot(pairs.astype(jnp.bfloat16), value, preferred_element_type=jnp.float32)
+    out += nt_dot((query * jnp.exp(run)).astype(jnp.bfloat16), state.astype(jnp.bfloat16))
+    mixed = head_norm(out, gain) * (gate * jax.nn.sigmoid(gate))
+    state = jnp.exp(last) * state + tn_dot(value, (key * jnp.exp(last - run)).astype(jnp.bfloat16))
+    return mixed.astype(jnp.bfloat16), state
+
+
+PARTS = 2
+
+
+def layer_kernel(n, *refs):
+    x_ref, e_ref, v_ref = refs[:3]
+    w_refs, o_refs = refs[3:10], refs[10:12]
+    out_ref, T = refs[12:14]
+    (
+        X, W, O, E, wp, proj, ma, mb, ts, M, away, landed,
+        x_send, x_recv, xx_send, xx_recv,
+        o_send, o_recv, oy_send, oy_recv, oc_send, oc_recv, od_send, od_recv,
+        w_send, w_recv, wy_send, wy_recv, wc_send, wc_recv, wd_send, wd_recv,
+        e_send, e_recv, m_send, m_recv, b_send, b_recv, t_send, t_recv, y_send, y_recv,
+        pack_sem, local_sem,
+    ) = refs[14:]
+    z, f, x = lax.axis_index("sp"), lax.axis_index("fs"), lax.axis_index("tp")
+    core, row, side = f + 1 - 2 * (f % 2), (f + 2) % 4, 1 - x
+    tokens = x_ref.shape[0]
+    half = tokens // 2
+    step = half // PARTS
+    both = (0, 1)
+
+    def cols(h):
+        return pl.ds(pl.multiple_of(h * HEAD, HEAD), HEAD)
+
+    packs = []
+    for i, w in enumerate(w_refs):
+        for h in range(n):
+            packs.append(
+                pltpu.make_async_copy(
+                    w.at[:, h * HEAD : (h + 1) * HEAD],
+                    wp.at[h, :, i * HEAD : (i + 1) * HEAD],
+                    pack_sem.at[i, h],
+                )
+            )
+    wide = o_refs[0].shape[1]
+    for i, o in enumerate(o_refs):
+        packs.append(
+            pltpu.make_async_copy(o, O.at[z, f, :, i * wide : (i + 1) * wide], local_sem.at[i])
+        )
+    for copy in packs:
+        copy.start()
+    local = [
+        pltpu.make_async_copy(x_ref, X.at[z], local_sem.at[2]),
+        pltpu.make_async_copy(e_ref.at[:, cols(z)], E.at[z], local_sem.at[3]),
+    ]
+    for copy in local:
+        copy.start()
+    greet(
+        [{"sp": (z + o) % n} for o in range(1, n)] + [{"fs": core}, {"fs": row}, {"tp": side}]
+    )
+
+    def reach(direction, k):
+        if direction == 0:
+            return (z - k >= 0) & (z + 1 < n), z - 1 - k >= 0, z - k, z - 1 - k, z + 1
+        return (z + k < n) & (z - 1 >= 0), z + 1 + k < n, z + k, z + 1 + k, z - 1
+
+    def span(c):
+        return pl.ds(pl.multiple_of(x * half + c * step, step), step)
+
+    def x_copy(direction, k, c, first=False):
+        _, _, out, _, to = reach(direction, k)
+        src = x_ref.at[span(c)] if first else X.at[out, span(c)]
+        return remote(
+            src, X.at[out, span(c)], x_send.at[direction, k, c], x_recv.at[direction, k, c], sp=to
+        )
+
+    def x_wait(direction, k, c):
+        block = X.at[reach(direction, k)[3], span(c)]
+        return remote(block, block, x_send.at[direction, k, c], x_recv.at[direction, k, c], sp=(z + 1) % n)
+
+    def xx_copy(direction, k, c):
+        block = X.at[reach(direction, k)[3], span(c)]
+        return remote(block, block, xx_send.at[direction, k, c], xx_recv.at[direction, k, c], tp=side)
+
+    def xx_wait(direction, k, c):
+        there = pl.ds(pl.multiple_of(side * half + c * step, step), step)
+        block = X.at[reach(direction, k)[3], there]
+        return remote(block, block, xx_send.at[direction, k, c], xx_recv.at[direction, k, c], tp=side)
+
+    def o_copy(direction, k):
+        _, _, out, _, to = reach(direction, k)
+        return remote(O.at[out, f], O.at[out, f], o_send.at[direction, k], o_recv.at[direction, k], sp=to)
+
+    def o_side(kind, direction, k, own=False):
+        block = z if own else reach(direction, k)[3]
+        send, recv = ((oy_send, oy_recv), (oc_send, oc_recv), (od_send, od_recv))[kind]
+        piece = O.at[block, row if kind == 2 else f]
+        where = {"fs": row if kind == 0 else core}
+        return remote(piece, piece, send.at[direction, k], recv.at[direction, k], **where)
+
+    def o_own(kind):
+        return o_side(kind, 2, 0, own=True)
+
+    def w_copy(o):
+        return remote(wp.at[(z + o) % n], W.at[z, f], w_send.at[o], w_recv.at[o], sp=(z + o) % n)
+
+    def e_copy(o):
+        return remote(e_ref.at[:, cols((z + o) % n)], E.at[z], e_send.at[o], e_recv.at[o], sp=(z + o) % n)
+
+    def w_side(kind, o):
+        block = (z - o + n) % n
+        src = wp.at[z] if o == 0 else W.at[block, f]
+        if kind == 0:
+            return remote(src, W.at[block, f], wy_send.at[o], wy_recv.at[o], fs=row)
+        if kind == 1:
+            return remote(src, W.at[block, f], wc_send.at[o], wc_recv.at[o], fs=core)
+        return remote(W.at[block, row], W.at[block, row], wd_send.at[o], wd_recv.at[o], fs=core)
+
+    for copy in packs:
+        copy.wait()
+    own_w = pltpu.make_async_copy(wp.at[z], W.at[z, f], local_sem.at[4])
+    own_w.start()
+    for o in range(1, n):
+        w_copy(o).start()
+    for kind in both:
+        w_side(kind, 0).start()
+    for d in both:
+        @pl.when(reach(d, 0)[0])
+        def _(d=d):
+            for c in range(PARTS):
+                x_copy(d, 0, c, True).start()
+    for o in range(1, n):
+        e_copy(o).start()
+    for o in range(1, n):
+        w_copy(o).wait_recv()
+        for kind in both:
+            w_side(kind, o).start()
+    for kind in both:
+        o_own(kind).start()
+    for copy in local:
+        copy.wait()
+    own_w.wait()
+
+    def project(block):
+        rows = X[block]
+        weights = W[...].reshape(rows.shape[1], W.shape[3])
+        made = jnp.dot(rows, weights, preferred_element_type=jnp.float32)
+        at = pl.ds(pl.multiple_of(block * tokens, tokens), tokens)
+        proj[at, :] = made.astype(jnp.bfloat16)
+
+    def gather_step(k, carry):
+        for d in both:
+            @pl.when((k < n - 1) & reach(d, k)[1])
+            def _(d=d):
+                for c in range(PARTS):
+                    x_wait(d, k, c).wait_recv()
+
+                    @pl.when(reach(d, k + 1)[0])
+                    def _(c=c):
+                        x_copy(d, k + 1, c).start()
+                    xx_copy(d, k, c).start()
+
+        @pl.when(k == max(n - 3, 0))
+        def _():
+            for d in both:
+                @pl.when(reach(d, 0)[0])
+                def _(d=d):
+                    o_copy(d, 0).start()
+
+        @pl.when(k == 0)
+        def _():
+            for o in range(n):
+                w_side(0, o).wait_recv()
+                w_side(2, o).start()
+            for o in range(n):
+                w_side(1, o).wait_recv()
+                w_side(2, o).wait_recv()
+
+        @pl.when(z - k >= 0)
+        def _():
+            @pl.when(k > 0)
+            def _():
+                for c in range(PARTS):
+                    xx_wait(0, k - 1, c).wait_recv()
+            project(z - k)
+
+        @pl.when((k > 0) & (z + k < n))
+        def _():
+            for c in range(PARTS):
+                xx_wait(1, k - 1, c).wait_recv()
+            project(z + k)
+        return carry
+
+    lax.fori_loop(0, n, gather_step, 0)
+
+    def o_tick(k):
+        for d in both:
+            @pl.when(reach(d, k)[1])
+            def _(d=d):
+                o_copy_in = O.at[reach(d, k)[3], f]
+                remote(o_copy_in, o_copy_in, o_send.at[d, k], o_recv.at[d, k], sp=(z + 1) % n).wait_recv()
+                if k + 1 < n - 1:
+                    @pl.when(reach(d, k + 1)[0])
+                    def _():
+                        o_copy(d, k + 1).start()
+                for kind in both:
+                    o_side(kind, d, k).start()
+
+    def m_copy(o):
+        return remote(ma.at[(z + o) % n], M.at[0, z], m_send.at[o], m_recv.at[o], sp=(z + o) % n)
+
+    def b_copy(o):
+        return remote(mb.at[(z + o) % n], M.at[1, z], b_send.at[o], b_recv.at[o], sp=(z + o) % n)
+
+    def t_copy(o):
+        return remote(ts.at[(z + o) % n], T.at[z], t_send.at[o], t_recv.at[o], sp=(z + o) % n)
+
+    param = lambda i: v_ref[i, pl.ds(z, 1), :]
+    shift = param(0)[:, 0:1]
+    for i in range(n):
+        mixed, keep = attend_tile(i, proj, shift, param(1))
+        ma[i] = mixed
+        total = jnp.log(jnp.maximum(1.0 - jnp.exp(keep), log_floor))
+        ts[i] = jnp.broadcast_to(total, (tokens, HEAD)).T[0:8, :]
+    o_tick(0)
+    for o in range(1, n):
+        e_copy(o).wait_recv()
+    floor, offset, gain = param(3), param(4), param(2)
+    per = tokens // CHUNK
+
+    def chunk(i, state):
+        here = pl.ds(pl.multiple_of(i * CHUNK, CHUNK), CHUNK)
+        at = pl.ds(pl.multiple_of((i % per) * CHUNK, CHUNK), CHUNK)
+        extra = E.at[i // per, at]
+        mixed, state = recur_chunk(proj, extra, here, state, floor, offset, gain)
+        mb[i // per, at, :] = mixed
+        return state
+
+    state = jnp.zeros((HEAD, HEAD), jnp.float32)
+    state = lax.fori_loop(0, per * n // 2, chunk, state)
+    for o in range(1, n):
+        m_copy(o).start()
+    for o in range(1, n):
+        t_copy(o).start()
+    if n > 2:
+        o_tick(1)
+    lax.fori_loop(per * n // 2, per * n, chunk, state)
+    for k in range(2, n - 1):
+        o_tick(k)
+    mine = [
+        pltpu.make_async_copy(ma.at[z], M.at[0, z], local_sem.at[5]),
+        pltpu.make_async_copy(mb.at[z], M.at[1, z], local_sem.at[6]),
+        pltpu.make_async_copy(ts.at[z], T.at[z], local_sem.at[7]),
+    ]
+    for o in range(1, n):
+        b_copy(o).start()
+    for copy in mine:
+        copy.start()
+    o_own(0).wait_recv()
+    o_own(2).start()
+    for k in range(n - 1):
+        for d in both:
+            @pl.when(reach(d, k)[1])
+            def _(d=d, k=k):
+                o_side(0, d, k).wait_recv()
+                o_side(2, d, k).start()
+    for copy in mine:
+        copy.wait()
+    for o in range(1, n):
+        m_copy(o).wait()
+        b_copy(o).wait()
+    o_own(1).wait_recv()
+    o_own(2).wait_recv()
+    for k in range(n - 1):
+        for d in both:
+            @pl.when(reach(d, k)[1])
+            def _(d=d, k=k):
+                o_side(1, d, k).wait_recv()
+                o_side(2, d, k).wait_recv()
+
+    def rows_of(which):
+        rows = pl.ds(pl.multiple_of(which * half, half), half)
+        return jnp.concatenate([M[g, k, rows, :] for g in both for k in range(n)], axis=1)
+
+    width = out_ref.shape[1] // n
+
+    def y_copy(j):
+        return remote(away.at[j], landed.at[j], y_send.at[j], y_recv.at[j], tp=side)
+
+    def weights_of(j):
+        return O[j].reshape(width, 2 * wide)
+
+    theirs = rows_of(side)
+    for j in range(n):
+        away[j] = nt_dot(theirs, weights_of(j)).astype(jnp.bfloat16)
+        if j:
+            y_copy(j - 1).start()
+    ours = rows_of(x)
+    for j in range(n):
+        piece = nt_dot(ours, weights_of(j))
+        if j == 0:
+            y_copy(n - 1).start()
+        y_copy(j).wait_recv()
+        piece += landed[j].astype(jnp.float32)
+        out_ref[:, j * width : (j + 1) * width] = piece.astype(jnp.bfloat16)
+    for j in range(n):
+        y_copy(j).wait_send()
+    for o in range(n):
+        for kind in range(3):
+            w_side(kind, o).wait_send()
+    for o in range(1, n):
+        t_copy(o).wait()
+        e_copy(o).wait_send()
+        w_copy(o).wait_send()
+    for kind in range(3):
+        o_own(kind).wait_send()
+    for k in range(n - 1):
+        for d in both:
+            @pl.when(reach(d, k)[1])
+            def _(d=d, k=k):
+                for c in range(PARTS):
+                    xx_copy(d, k, c).wait_send()
+                for kind in range(3):
+                    o_side(kind, d, k).wait_send()
+
+            @pl.when(reach(d, k)[0])
+            def _(d=d, k=k):
+                for c in range(PARTS):
+                    x_copy(d, k, c).wait_send()
+                o_copy(d, k).wait_send()
+
+
+VMEM = pl.BlockSpec(memory_space=pltpu.VMEM)
+ANY = pl.BlockSpec(memory_space=pl.ANY)
+DMA = pltpu.SemaphoreType.DMA
+
+
+def on_device_heads(
+    n,
+    input_layer_rows,
+    input_norm_gain,
+    query_weight_attention,
+    key_weight_attention,
+    value_weight_attention,
+    query_weight_recurrent,
+    forget_weight_recurrent,
+    value_weight_recurrent,
+    gate_weight_recurrent,
+    output_weight_attention,
+    emitted_projection_linear_scan,
+    score_offset,
+    attention_norm_gain,
+    recurrence_norm_gain,
+    forget_floor,
+    forget_offset,
+    extra_log_decay,
+):
+    values = input_layer_rows[0].astype(jnp.float32)
+    square_mean = jnp.mean(values * values, axis=-1, keepdims=True)
+    normed = (values * lax.rsqrt(square_mean + epsilon) * input_norm_gain).astype(jnp.bfloat16)
+    tokens, depth = normed.shape
+    groups = lax.axis_size("fs")
+    share, columns = query_weight_attention.shape
+    width = 7 * HEAD
+    half = tokens // 2
+    vectors = jnp.stack(
+        [jnp.broadcast_to(score_offset[:, None], (n, HEAD))]
+        + [
+            v.reshape(n, HEAD)
+            for v in (attention_norm_gain, recurrence_norm_gain, forget_floor, forget_offset)
+        ]
+    )
+    bf = lambda *shape: pltpu.VMEM(shape, jnp.bfloat16)
+    layer_out, T = pl.pallas_call(
+        functools.partial(layer_kernel, n),
+        out_shape=(
+            jax.ShapeDtypeStruct((half, depth), jnp.bfloat16),
+            jax.ShapeDtypeStruct((n, 8, tokens), jnp.float32),
+        ),
+        in_specs=[VMEM] * 3 + [ANY] * 9,
+        out_specs=(VMEM,) * 2,
+        scratch_shapes=[
+            bf(n, tokens, depth),
+            bf(n, groups, share, width),
+            bf(n, groups, share, 2 * columns),
+            bf(n, tokens, HEAD),
+            bf(n, share, width),
+            bf(n * tokens, width),
+            bf(n, tokens, HEAD),
+            bf(n, tokens, HEAD),
+            pltpu.VMEM((n, 8, tokens), jnp.float32),
+            bf(2, n, tokens, HEAD),
+            bf(n, half, depth // n),
+            bf(n, half, depth // n),
+        ]
+        + [DMA((2, n, PARTS))] * 4
+        + [DMA((2, n))] * 2
+        + [DMA((3, n))] * 6
+        + [DMA((n,))] * 18
+        + [DMA((7, n)), DMA((8,))],
+        compiler_params=pltpu.CompilerParams(
+            collective_id=0, has_side_effects=True, vmem_limit_bytes=56 * 1024 * 1024
+        ),
+    )(
+        normed,
+        extra_log_decay[0].astype(jnp.bfloat16),
+        vectors,
+        query_weight_attention,
+        key_weight_attention,
+        value_weight_attention,
+        query_weight_recurrent,
+        forget_weight_recurrent,
+        value_weight_recurrent,
+        gate_weight_recurrent,
+        output_weight_attention,
+        emitted_projection_linear_scan,
+    )
+    return (layer_out[None], T[:, 0, :][None])
+
+
 def solution(mesh):
+    n = mesh.shape["sp"]
+    heads_fit = mesh.shape["fs"] == 4 and mesh.shape["tp"] == 2 and n > 1
+
+    def on_device(*args):
+        if heads_fit and args[11].shape[0] == n and args[0].shape[1] == TILE:
+            return on_device_heads(n, *args)
+        return on_device_general(*args)
+
     return jax.shard_map(
         on_device,
         mesh=mesh,

time: 480 us -> 126 us (0.26); the launches traced: 473 us -> 126 us
  waiting for transfers between devices: 301 us -> 0 us
  Pallas kernels: 0 us -> 116 us
  other arithmetic: 66.7 us -> 4.65 us
  matrix products: 43.6 us -> 0 us
  blocking collectives: 29.3 us -> 0 us
  between operations: 14.7 us -> 0.73 us
  loops' own time: 11.9 us -> 0 us
    all_gather x10 -> x0, waiting for transfers between devices: 277 us -> none  [the longest x1 40.9 us: on_device(): lax.all_gather(weights_in[1], ('sp', 'fs'), axis=0, tiled=True)]
    pallas_call x0 -> x1, Pallas kernels: none -> 116 us  [on_device_heads(): pl.pallas_call(functools.partial(layer_kernel, n), out_shape=(jax.ShapeDt...]
    dot_general x30 -> x0, matrix products: 43.6 us -> none  [the longest x7 18.5 us: on_device(): jnp.dot(normed, weight, preferred_element_type=jnp.float32)]
    another operation x19 -> x0, other arithmetic: 40 us -> none
    all_gather x2 -> x0, blocking collectives: 29.3 us -> none  [entering(): lax.all_gather(part.astype(kind), axis)]
    reduce_scatter x1 -> x0, waiting for transfers between devices: 18.6 us -> none  [on_device(): lax.psum_scatter((contract_rows(mixed_a, out_a) + contract_rows(mixed_b,...]
    reduce_sum x7 -> x1, other arithmetic: 17.2 us -> 1.59 us  [on_device_heads(): square_mean = jnp.mean(values * values, axis=-1, keepdims=True)]
    another operation x3 -> x0, loops' own time: 11.9 us -> none  [the longest x1 11.4 us: entering(): return lax.fori_loop(0, size, hop, start)]
  transfers between devices with their start and end apart: 11 -> 0, of which waited for: 9 -> 0; matrix products, arithmetic and copies ran while one was open for 23% -> 0% of each run, Pallas kernels for 0% -> 0%
where the time goes in v2:
time: 126 us
  Pallas kernels  116 us (92%)
  other arithmetic  4.65 us (4%)
  local copies, waits for them, and re-layouts  4.03 us (3%)
    pallas_call x1, Pallas kernels, on_device_heads(): pl.pallas_call(functools.partial(layer_kernel, n), out_shape=(jax.ShapeDt...  116 us
    unnamed x20, local copies, waits for them, and re-layouts  3.26 us

profile of v2, /device:TPU:0, one launch (start us, length us, event | category | flops | bytes accessed | tf_op | source)
XLA Modules:
  0.0 125.6 jit_solution(11480416206368826311)
XLA Ops:
  0.6 0.0 copy-start
  0.6 0.0 copy-start.4
  0.7 0.0 copy-start.3
  0.7 0.0 copy-start.5
  0.7 0.0 copy-start.6
  0.7 0.0 copy-start.2
  0.7 1.6 %fusion = f32[256]{0:T(256)S(1)} fusion(bf16[1,256,2048]{2,1,0:T(8,128)(2,1)} %param.17), kind=kLoop, calls=%fused_computation.2 | loop fusion | flops 1572608 | bytes 1049600 | tf_op jit(solution)/shard_map/reduce_sum | solution.py:672
  2.3 0.7 constant_dynamic-update-slice_fusion.4
  3.0 0.0 copy-done.3
  3.0 0.0 copy-done.4
  3.0 0.0 copy-done.5
  3.1 0.0 copy-done.6
  3.1 0.0 copy-start.1
  3.1 1.8 %convert_bitcast_fusion.refs_1_ = bf16[256,512]{1,0:T(8,128)(2,1)} fusion(f32[1,256,512]{2,1,0:T(8,128)} %param.33), kind=kLoop, calls=%fused_computation.5 | loop fusion | flops 131072 | bytes 786432 | tf_op jit(solution)/shard_map/convert_element_type | solution.py:719
  4.9 0.0 copy-done
  4.9 0.0 copy-done.2
  4.9 1.3 %fusion.2.refs_0_ = bf16[256,2048]{1,0:T(8,128)(2,1)} fusion(bf16[1,256,2048]{2,1,0:T(8,128)(2,1)S(1)} %copy-done, f32[2048]{0:T(1024)S(1)} %copy-done.2, f32[256]{0:T(256)S(1)} %add_rsqrt_fusion), kind=kLoop, calls=%fused_computation.4 | loop fusion | flops 2097152 | bytes 2106368 | tf_op jit(solution)/shard_map/convert_element_type | solution.py:673
  6.2 0.0 copy-done.1
  6.2 116.2 %shard_map.176 = (bf16[128,2048]{1,0:T(8,128)(2,1)}, f32[4,8,256]{2,1,0:T(8,128)}) custom-call(bf16[256,2048]{1,0:T(8,128)(2,1)} %fusion.2.refs_0_, bf16[256,512]{1,0:T(8,128)(2,1)} %convert_bitcast_fusion.refs_1_, f32[5,4,128]{2,1,0:T(4,128)} %copy-done.1, bf16[128,512]{1,0:T(8,128)(2,1)} %refs_3_.1, bf16[128,512]{1,0:T(8,128)(2,1)} %refs_4_.1, ...), custom_call_target="tpu_custom_call" | custom-call | tf_op jit(solution)/shard_map/pallas_call | solution.py:687
  122.3 0.8 slice_bitcast_fusion
  123.1 0.6 copy.19
  123.7 1.9 %copy.25 = bf16[1,128,2048]{2,1,0:T(8,128)(2,1)} copy(bf16[1,128,2048]{2,1,0:T(8,128)(2,1)} %bitcast.17) | data formatting | bytes 1048576
  (5 shorter events, 0.0 us)
Async XLA Ops:
  0.6 4.2 %copy-start = (bf16[1,256,2048]{2,1,0:T(8,128)(2,1)S(1)}, bf16[1,256,2048]{2,1,0:T(8,128)(2,1)}, u32[]{:S(2)}) copy-start(bf16[1,256,2048]{2,1,0:T(8,128)(2,1)} %param.17) | copy-start | bytes 3145732
  0.6 2.4 %copy-start.4 = (f32[512]{0:T(512)S(1)}, f32[512]{0:T(512)}, u32[]{:S(2)}) copy-start(f32[512]{0:T(512)} %param.30) | copy-start | bytes 6148
  0.7 2.4 %copy-start.3 = (f32[512]{0:T(512)S(1)}, f32[512]{0:T(512)}, u32[]{:S(2)}) copy-start(f32[512]{0:T(512)} %param.29) | copy-start | bytes 6148
  0.7 2.4 %copy-start.5 = (f32[512]{0:T(512)S(1)}, f32[512]{0:T(512)}, u32[]{:S(2)}) copy-start(f32[512]{0:T(512)} %param.31) | copy-start | bytes 6148
  0.7 2.4 %copy-start.6 = (f32[512]{0:T(512)S(1)}, f32[512]{0:T(512)}, u32[]{:S(2)}) copy-start(f32[512]{0:T(512)} %param.32) | copy-start | bytes 6148
  0.7 4.2 %copy-start.2 = (f32[2048]{0:T(1024)S(1)}, f32[2048]{0:T(1024)}, u32[]{:S(2)}) copy-start(f32[2048]{0:T(1024)} %param.18) | copy-start | bytes 24580
  3.1 3.1 %copy-start.1 = (f32[5,4,128]{2,1,0:T(4,128)}, f32[5,4,128]{2,1,0:T(4,128)S(1)}, u32[]{:S(2)}) copy-start(f32[5,4,128]{2,1,0:T(4,128)S(1)} %constant_dynamic-update-slice_fusion.refs_2_) | copy-start | bytes 30724

commit v3 on v2

--- a/solution.py
+++ b/solution.py
@@ -320,21 +320,21 @@
     return mixed.astype(jnp.bfloat16), state
 
 
-PARTS = 2
+PARTS = 4
 
 
 def layer_kernel(n, *refs):
-    x_ref, e_ref, v_ref = refs[:3]
-    w_refs, o_refs = refs[3:10], refs[10:12]
-    out_ref, T = refs[12:14]
+    raw_ref, g_ref, xe_ref, v_ref = refs[:4]
+    w_refs, o_refs = refs[4:11], refs[11:13]
+    out_ref, T = refs[13:15]
     (
-        X, W, O, E, wp, proj, ma, mb, ts, M, away, landed,
+        X, W, O, E, x_ref, e_ref, wp, proj, ma, mb, ts, M, away, landed,
         x_send, x_recv, xx_send, xx_recv,
         o_send, o_recv, oy_send, oy_recv, oc_send, oc_recv, od_send, od_recv,
         w_send, w_recv, wy_send, wy_recv, wc_send, wc_recv, wd_send, wd_recv,
         e_send, e_recv, m_send, m_recv, b_send, b_recv, t_send, t_recv, y_send, y_recv,
         pack_sem, local_sem,
-    ) = refs[14:]
+    ) = refs[15:]
     z, f, x = lax.axis_index("sp"), lax.axis_index("fs"), lax.axis_index("tp")
     core, row, side = f + 1 - 2 * (f % 2), (f + 2) % 4, 1 - x
     tokens = x_ref.shape[0]
@@ -362,15 +362,22 @@
         )
     for copy in packs:
         copy.start()
-    local = [
-        pltpu.make_async_copy(x_ref, X.at[z], local_sem.at[2]),
-        pltpu.make_async_copy(e_ref.at[:, cols(z)], E.at[z], local_sem.at[3]),
-    ]
-    for copy in local:
-        copy.start()
-    greet(
-        [{"sp": (z + o) % n} for o in range(1, n)] + [{"fs": core}, {"fs": row}, {"tp": side}]
-    )
+    barrier = pltpu.get_barrier_semaphore()
+    peers = [{"sp": (z + o) % n} for o in range(1, n)] + [{"fs": core}, {"fs": row}, {"tp": side}]
+    for where in peers:
+        pl.semaphore_signal(barrier, inc=1, device_id=where, device_id_type=MESH)
+
+    def normalise(i, carry):
+        rows = pl.ds(pl.multiple_of(i * step, step), step)
+        x_ref[rows, :] = head_norm(raw_ref[rows, :].astype(jnp.float32), g_ref[...]).astype(jnp.bfloat16)
+        return carry
+
+    lax.fori_loop(0, tokens // step, normalise, 0)
+    for copy in packs:
+        copy.wait()
+    pl.semaphore_wait(barrier, len(peers))
+    own_w = pltpu.make_async_copy(wp.at[z], W.at[z, f], local_sem.at[4])
+    own_w.start()
 
     def reach(direction, k):
         if direction == 0:
@@ -429,29 +436,30 @@
             return remote(src, W.at[block, f], wc_send.at[o], wc_recv.at[o], fs=core)
         return remote(W.at[block, row], W.at[block, row], wd_send.at[o], wd_recv.at[o], fs=core)
 
-    for copy in packs:
-        copy.wait()
-    own_w = pltpu.make_async_copy(wp.at[z], W.at[z, f], local_sem.at[4])
-    own_w.start()
-    for o in range(1, n):
-        w_copy(o).start()
-    for kind in both:
-        w_side(kind, 0).start()
     for d in both:
         @pl.when(reach(d, 0)[0])
         def _(d=d):
             for c in range(PARTS):
                 x_copy(d, 0, c, True).start()
     for o in range(1, n):
-        e_copy(o).start()
-    for o in range(1, n):
-        w_copy(o).wait_recv()
-        for kind in both:
-            w_side(kind, o).start()
+        w_copy(o).start()
     for kind in both:
-        o_own(kind).start()
-    for copy in local:
-        copy.wait()
+        w_side(kind, 0).start()
+    local = [
+        pltpu.make_async_copy(x_ref, X.at[z], local_sem.at[2]),
+        pltpu.make_async_copy(e_ref.at[:, cols(z)], E.at[z], local_sem.at[3]),
+    ]
+    local[0].start()
+    e_ref[...] = xe_ref[...].astype(jnp.bfloat16)
+
+    def o_begin(direction, when):
+        @pl.when(when & reach(direction, 0)[0])
+        def _():
+            o_copy(direction, 0).start()
+
+    o_begin(0, z == 0)
+    o_begin(1, z == n - 1)
+    local[0].wait()
     own_w.wait()
 
     def project(block):
@@ -475,13 +483,21 @@
 
         @pl.when(k == max(n - 3, 0))
         def _():
-            for d in both:
-                @pl.when(reach(d, 0)[0])
-                def _(d=d):
-                    o_copy(d, 0).start()
+            local[1].start()
+            for o in range(1, n):
+                e_copy(o).start()
+
+        o_begin(0, (z > 0) & (k == z - 1))
+        o_begin(1, (z < n - 1) & (k == n - 2 - z))
 
         @pl.when(k == 0)
         def _():
+            for o in range(1, n):
+                w_copy(o).wait_recv()
+                for kind in both:
+                    w_side(kind, o).start()
+            for kind in both:
+                o_own(kind).start()
             for o in range(n):
                 w_side(0, o).wait_recv()
                 w_side(2, o).start()
@@ -528,6 +544,7 @@
     def t_copy(o):
         return remote(ts.at[(z + o) % n], T.at[z], t_send.at[o], t_recv.at[o], sp=(z + o) % n)
 
+    o_tick(0)
     param = lambda i: v_ref[i, pl.ds(z, 1), :]
     shift = param(0)[:, 0:1]
     for i in range(n):
@@ -535,7 +552,7 @@
         ma[i] = mixed
         total = jnp.log(jnp.maximum(1.0 - jnp.exp(keep), log_floor))
         ts[i] = jnp.broadcast_to(total, (tokens, HEAD)).T[0:8, :]
-    o_tick(0)
+    local[1].wait()
     for o in range(1, n):
         e_copy(o).wait_recv()
     floor, offset, gain = param(3), param(4), param(2)
@@ -550,46 +567,51 @@
         return state
 
     state = jnp.zeros((HEAD, HEAD), jnp.float32)
-    state = lax.fori_loop(0, per * n // 2, chunk, state)
+    count = per * n
+    state = lax.fori_loop(0, count // 4, chunk, state)
     for o in range(1, n):
         m_copy(o).start()
     for o in range(1, n):
         t_copy(o).start()
     if n > 2:
         o_tick(1)
-    lax.fori_loop(per * n // 2, per * n, chunk, state)
-    for k in range(2, n - 1):
-        o_tick(k)
+    lax.fori_loop(count // 4, count, chunk, state)
     mine = [
         pltpu.make_async_copy(ma.at[z], M.at[0, z], local_sem.at[5]),
         pltpu.make_async_copy(mb.at[z], M.at[1, z], local_sem.at[6]),
         pltpu.make_async_copy(ts.at[z], T.at[z], local_sem.at[7]),
     ]
+    for copy in mine:
+        copy.start()
     for o in range(1, n):
         b_copy(o).start()
-    for copy in mine:
-        copy.start()
     o_own(0).wait_recv()
     o_own(2).start()
-    for k in range(n - 1):
-        for d in both:
-            @pl.when(reach(d, k)[1])
-            def _(d=d, k=k):
-                o_side(0, d, k).wait_recv()
-                o_side(2, d, k).start()
+    for k in range(2, n - 1):
+        o_tick(k)
+    o_own(1).wait_recv()
+    o_own(2).wait_recv()
     for copy in mine:
         copy.wait()
     for o in range(1, n):
         m_copy(o).wait()
         b_copy(o).wait()
-    o_own(1).wait_recv()
-    o_own(2).wait_recv()
-    for k in range(n - 1):
-        for d in both:
-            @pl.when(reach(d, k)[1])
-            def _(d=d, k=k):
-                o_side(1, d, k).wait_recv()
-                o_side(2, d, k).wait_recv()
+
+    shorter = jnp.minimum(z, n - 1 - z)
+
+    def hop_of(s):
+        t = s - 1
+        paired = t < 2 * shorter
+        k = jnp.where(paired, t // 2, t - shorter)
+        d = jnp.where(paired, t % 2, jnp.where(z > n - 1 - z, 0, 1))
+        return d, k, jnp.where(d == 0, z - 1 - k, z + 1 + k)
+
+    def o_late(kind, s):
+        d, k, block = hop_of(s)
+        send, recv = ((oy_send, oy_recv), (oc_send, oc_recv), (od_send, od_recv))[kind]
+        piece = O.at[block, row if kind == 2 else f]
+        where = {"fs": row if kind == 0 else core}
+        return remote(piece, piece, send.at[d, k], recv.at[d, k], **where)
 
     def rows_of(which):
         rows = pl.ds(pl.multiple_of(which * half, half), half)
@@ -600,22 +622,31 @@
     def y_copy(j):
         return remote(away.at[j], landed.at[j], y_send.at[j], y_recv.at[j], tp=side)
 
-    def weights_of(j):
-        return O[j].reshape(width, 2 * wide)
+    def weights_of(block):
+        return O[block].reshape(width, 2 * wide)
 
     theirs = rows_of(side)
+    o_late(0, 1).wait_recv()
+    o_late(2, 1).start()
     for j in range(n):
-        away[j] = nt_dot(theirs, weights_of(j)).astype(jnp.bfloat16)
+        if j:
+            o_late(1, j).wait_recv()
+            o_late(2, j).wait_recv()
+        away[j] = nt_dot(theirs, weights_of(hop_of(j)[2] if j else z)).astype(jnp.bfloat16)
         if j:
             y_copy(j - 1).start()
+            if j + 1 < n:
+                o_late(0, j + 1).wait_recv()
+                o_late(2, j + 1).start()
     ours = rows_of(x)
     for j in range(n):
-        piece = nt_dot(ours, weights_of(j))
+        block = hop_of(j)[2] if j else z
+        piece = nt_dot(ours, weights_of(block))
         if j == 0:
             y_copy(n - 1).start()
         y_copy(j).wait_recv()
         piece += landed[j].astype(jnp.float32)
-        out_ref[:, j * width : (j + 1) * width] = piece.astype(jnp.bfloat16)
+        out_ref[:, pl.ds(pl.multiple_of(block * width, width), width)] = piece.astype(jnp.bfloat16)
     for j in range(n):
         y_copy(j).wait_send()
     for o in range(n):
@@ -668,10 +699,7 @@
     forget_offset,
     extra_log_decay,
 ):
-    values = input_layer_rows[0].astype(jnp.float32)
-    square_mean = jnp.mean(values * values, axis=-1, keepdims=True)
-    normed = (values * lax.rsqrt(square_mean + epsilon) * input_norm_gain).astype(jnp.bfloat16)
-    tokens, depth = normed.shape
+    _, tokens, depth = input_layer_rows.shape
     groups = lax.axis_size("fs")
     share, columns = query_weight_attention.shape
     width = 7 * HEAD
@@ -690,13 +718,15 @@
             jax.ShapeDtypeStruct((half, depth), jnp.bfloat16),
             jax.ShapeDtypeStruct((n, 8, tokens), jnp.float32),
         ),
-        in_specs=[VMEM] * 3 + [ANY] * 9,
+        in_specs=[VMEM] * 4 + [ANY] * 9,
         out_specs=(VMEM,) * 2,
         scratch_shapes=[
             bf(n, tokens, depth),
             bf(n, groups, share, width),
             bf(n, groups, share, 2 * columns),
             bf(n, tokens, HEAD),
+            bf(tokens, depth),
+            bf(tokens, columns),
             bf(n, share, width),
             bf(n * tokens, width),
             bf(n, tokens, HEAD),
@@ -715,8 +745,9 @@
             collective_id=0, has_side_effects=True, vmem_limit_bytes=56 * 1024 * 1024
         ),
     )(
-        normed,
-        extra_log_decay[0].astype(jnp.bfloat16),
+        input_layer_rows[0],
+        input_norm_gain[None],
+        extra_log_decay[0],
         vectors,
         query_weight_attention,
         key_weight_attention,

time: 126 us -> 123 us (0.976)
  other arithmetic: 4.65 us -> 0 us
  local copies, waits for them, and re-layouts: 4.03 us -> 6.6 us
    convert_element_type x2 -> x0, other arithmetic: 3.06 us -> none  [the longest x1 1.78 us: on_device_heads(): extra_log_decay[0].astype(jnp.bfloat16)]
    unnamed x20 -> x18, local copies, waits for them, and re-layouts: 3.26 us -> 5.83 us
    reduce_sum x1 -> x0, other arithmetic: 1.59 us -> none  [on_device_heads(): square_mean = jnp.mean(values * values, axis=-1, keepdims=True)]
where the time goes in v3:
time: 123 us
  Pallas kernels  116 us (94%)
  local copies, waits for them, and re-layouts  6.6 us (5%)
    pallas_call x1, Pallas kernels, on_device_heads(): pl.pallas_call(functools.partial(layer_kernel, n), out_shape=(jax.ShapeDt...  116 us
    unnamed x18, local copies, waits for them, and re-layouts  5.83 us

profile of v3, /device:TPU:0, one launch (start us, length us, event | category | flops | bytes accessed | tf_op | source)
XLA Modules:
  0.0 122.8 jit_solution(1717661182295609130)
XLA Ops:
  0.6 0.0 copy-start.5
  0.6 0.0 copy-start.1
  0.6 0.6 copy-done.5
  1.3 0.1 constant_dynamic-update-slice_fusion.4
  1.4 0.0 copy-done.1
  1.4 0.0 copy-start.2
  1.4 0.7 copy-done.2
  2.0 0.0 copy-start.3
  2.1 0.7 copy-done.3
  2.7 0.0 copy-start.4
  2.7 0.7 copy-done.4
  3.4 0.0 copy-start
  3.4 0.6 copy-done
  4.0 115.5 %shard_map.176 = (bf16[128,2048]{1,0:T(8,128)(2,1)}, f32[4,8,256]{2,1,0:T(8,128)}) custom-call(bf16[256,2048]{1,0:T(8,128)(2,1)} %bitcast.14, f32[1,2048]{1,0:T(1,128)} %bitcast.17, f32[256,512]{1,0:T(8,128)} %bitcast.16, f32[5,4,128]{2,1,0:T(4,128)} %copy-done, bf16[128,512]{1,0:T(8,128)(2,1)} %refs_4_.1, bf16[128,512]{1,0:T(8,128)(2,1)} %refs_5_.1, ...), custom_call_target="tpu_custom_call" | custom-call | tf_op jit(solution)/shard_map/pallas_call | solution.py:715
  119.5 0.8 slice_bitcast_fusion
  120.3 0.6 copy.19
  120.9 1.9 %copy.25 = bf16[1,128,2048]{2,1,0:T(8,128)(2,1)} copy(bf16[1,128,2048]{2,1,0:T(8,128)(2,1)} %bitcast.15) | data formatting | bytes 1048576
  (4 shorter events, 0.0 us)
Async XLA Ops:
  0.6 0.7 copy-start.5
  0.6 0.7 copy-start.1
  1.4 0.7 copy-start.2
  2.0 0.7 copy-start.3
  2.7 0.7 copy-start.4
  3.4 0.6 copy-start

commit v4 on v3

--- a/solution.py
+++ b/solution.py
@@ -457,8 +457,6 @@
         def _():
             o_copy(direction, 0).start()
 
-    o_begin(0, z == 0)
-    o_begin(1, z == n - 1)
     local[0].wait()
     own_w.wait()
 
@@ -481,14 +479,14 @@
                         x_copy(d, k + 1, c).start()
                     xx_copy(d, k, c).start()
 
-        @pl.when(k == max(n - 3, 0))
+        @pl.when(k == n - 2)
         def _():
             local[1].start()
             for o in range(1, n):
                 e_copy(o).start()
 
-        o_begin(0, (z > 0) & (k == z - 1))
-        o_begin(1, (z < n - 1) & (k == n - 2 - z))
+        o_begin(0, k == n - 2)
+        o_begin(1, k == n - 2)
 
         @pl.when(k == 0)
         def _():
@@ -544,7 +542,6 @@
     def t_copy(o):
         return remote(ts.at[(z + o) % n], T.at[z], t_send.at[o], t_recv.at[o], sp=(z + o) % n)
 
-    o_tick(0)
     param = lambda i: v_ref[i, pl.ds(z, 1), :]
     shift = param(0)[:, 0:1]
     for i in range(n):
@@ -552,6 +549,7 @@
         ma[i] = mixed
         total = jnp.log(jnp.maximum(1.0 - jnp.exp(keep), log_floor))
         ts[i] = jnp.broadcast_to(total, (tokens, HEAD)).T[0:8, :]
+    o_tick(0)
     local[1].wait()
     for o in range(1, n):
         e_copy(o).wait_recv()
@@ -568,14 +566,14 @@
 
     state = jnp.zeros((HEAD, HEAD), jnp.float32)
     count = per * n
-    state = lax.fori_loop(0, count // 4, chunk, state)
+    state = lax.fori_loop(0, count // 2, chunk, state)
     for o in range(1, n):
         m_copy(o).start()
     for o in range(1, n):
         t_copy(o).start()
     if n > 2:
         o_tick(1)
-    lax.fori_loop(count // 4, count, chunk, state)
+    lax.fori_loop(count // 2, count, chunk, state)
     mine = [
         pltpu.make_async_copy(ma.at[z], M.at[0, z], local_sem.at[5]),
         pltpu.make_async_copy(mb.at[z], M.at[1, z], local_sem.at[6]),

time: 123 us -> 125 us (1.016)
    pallas_call x1, Pallas kernels: 116 us -> 117 us  [on_device_heads(): pl.pallas_call(functools.partial(layer_kernel, n), out_shape=(jax.ShapeDt...]
where the time goes in v4:
time: 125 us; the launch traced here: 124 us
  Pallas kernels  117 us (94%)
  local copies, waits for them, and re-layouts  6.6 us (5%)
    pallas_call x1, Pallas kernels, on_device_heads(): pl.pallas_call(functools.partial(layer_kernel, n), out_shape=(jax.ShapeDt...  117 us
    unnamed x18, local copies, waits for them, and re-layouts  5.83 us

profile of v4, /device:TPU:0, one launch (start us, length us, event | category | flops | bytes accessed | tf_op | source)
XLA Modules:
  0.0 124.4 jit_solution(10180190384776300598)
XLA Ops:
  0.6 0.0 copy-start.5
  0.6 0.0 copy-start.1
  0.6 0.6 copy-done.5
  1.3 0.1 constant_dynamic-update-slice_fusion.4
  1.4 0.0 copy-done.1
  1.4 0.0 copy-start.2
  1.4 0.7 copy-done.2
  2.0 0.0 copy-start.3
  2.1 0.7 copy-done.3
  2.7 0.0 copy-start.4
  2.7 0.7 copy-done.4
  3.4 0.0 copy-start
  3.4 0.6 copy-done
  4.0 117.1 %shard_map.176 = (bf16[128,2048]{1,0:T(8,128)(2,1)}, f32[4,8,256]{2,1,0:T(8,128)}) custom-call(bf16[256,2048]{1,0:T(8,128)(2,1)} %bitcast.14, f32[1,2048]{1,0:T(1,128)} %bitcast.17, f32[256,512]{1,0:T(8,128)} %bitcast.16, f32[5,4,128]{2,1,0:T(4,128)} %copy-done, bf16[128,512]{1,0:T(8,128)(2,1)} %refs_4_.1, bf16[128,512]{1,0:T(8,128)(2,1)} %refs_5_.1, ...), custom_call_target="tpu_custom_call" | custom-call | tf_op jit(solution)/shard_map/pallas_call | solution.py:713
  121.2 0.8 slice_bitcast_fusion
  121.9 0.6 copy.19
  122.5 1.9 %copy.25 = bf16[1,128,2048]{2,1,0:T(8,128)(2,1)} copy(bf16[1,128,2048]{2,1,0:T(8,128)(2,1)} %bitcast.15) | data formatting | bytes 1048576
  (4 shorter events, 0.0 us)
Async XLA Ops:
  0.6 0.7 copy-start.5
  0.6 0.7 copy-start.1
  1.4 0.7 copy-start.2
  2.0 0.7 copy-start.3
  2.7 0.7 copy-start.4
  3.4 0.6 copy-start
